TPU v7x, 32 devices: a whole 2x2x4 slice. The times are simulated.
32 devices in a mesh: sp: 8 (over z, y), tp: 4 (over x, core).
Axes of the slice: x: 2, y: 2, z: 4, core: 2. Of those that a mesh axis runs over, the one named last changes fastest.
Arguments:
- skip_stream_vector: bfloat16 [8192, 2048], P(('sp', 'tp')), may hold values from -6 to 6
- probe_preactivation: bfloat16 [8192, 1024], P('sp', 'tp'), may hold values from -6 to 6
- retention_preactivation: bfloat16 [8192, 1024], P('sp', 'tp'), may hold values from -4.5 to 4.5
- content_vector: bfloat16 [8192, 1024], P('sp', 'tp'), may hold values from -6 to 6
- emission_preactivation: bfloat16 [8192, 1024], P('sp', 'tp'), may hold values from -6 to 6
- retention_slack: float32 [1024], P('tp'), may hold values from 0 to 0.12
- surge_rate: float32 [8192, 1024], P('sp', 'tp'), may hold values from -1.2 to 0
- subspace_scaling_factor: float32 [1024], P('tp'), may hold values from 0.1 to 1.9
- emission_matrix: bfloat16 [1024, 2048], replicated, may hold values from -0.1875 to 0.1875
- mlp_scaling_factor: float32 [2048], replicated, may hold values from 0.1 to 1.9
- switch_matrix: bfloat16 [2048, 5632], P('sp', 'tp'), may hold values from -0.125 to 0.125
- expansion_matrix: bfloat16 [2048, 5632], P('sp', 'tp'), may hold values from -0.125 to 0.125
- contraction_matrix: bfloat16 [5632, 2048], P('tp', 'sp'), may hold values from -0.078125 to 0.078125
Outputs:
- stream_out: bfloat16 [8192, 2048], P(('sp', 'tp'))
All inputs are finite; a program needn't handle non-finite values.
Results may differ from a plain program's by a relative error of at most 0.017.
Values may be sent and summed in bfloat16 or wider, within the bound.
No kernel may reach another device: no remote copies, remote signals or barrier semaphores. Data moves between devices by JAX's collectives and lax.ppermute only.
A program may use at most 128 MiB of HBM per device.

v0:
```python
import functools

import jax
import jax.numpy as jnp
from jax import lax
from jax.experimental import pallas as pl
from jax.experimental.pallas import tpu as pltpu
from jax.sharding import Mesh
from jax.sharding import PartitionSpec as P


HEAD_DIM = 128
BLOCK = 64
CHUNK = 512
EPSILON = 1e-06
F32 = jnp.float32
BF16 = jnp.bfloat16
ANY = pl.BlockSpec(memory_space=pltpu.HBM)
VMEM = pl.BlockSpec(memory_space=pltpu.VMEM)


NN = (((1,), (0,)), ((), ()))
NT = (((1,), (1,)), ((), ()))
TN = (((0,), (0,)), ((), ()))


def dot(a, b, dims=NN):
    return lax.dot_general(a, b, dims, preferred_element_type=F32)


def parts(a):
    high = a.astype(BF16)
    return high, (a - high.astype(F32)).astype(BF16)


def dot_split(a, b, dims):
    a_high, a_low = parts(a)
    b_high, b_low = parts(b)
    return dot(a_high, b_high, dims) + (dot(a_high, b_low, dims) + dot(a_low, b_high, dims))


def scan_kernel(probe, retention, content, slack, surge, out, carried, message, state, offset):
    rows, width = probe.shape
    heads = width // HEAD_DIM
    state[...] = jnp.zeros_like(state)
    offset[...] = jnp.zeros_like(offset)
    first = lax.broadcasted_iota(jnp.int32, (BLOCK, BLOCK), 0)
    second = lax.broadcasted_iota(jnp.int32, (BLOCK, BLOCK), 1)
    causal = first >= second
    ones = jnp.where(causal, 1.0, 0.0).astype(BF16)

    def step(turn, _):
        here = pl.ds(pl.multiple_of(turn * BLOCK, BLOCK), BLOCK)
        before = probe[here, :].astype(F32)
        query = before * jax.nn.sigmoid(before)
        gate = slack[...] * jax.nn.sigmoid(-retention[here, :].astype(F32))
        rate = jnp.log1p(-gate) + surge[here, :]
        value = content[here, :]
        high = rate.astype(BF16)
        rest = rate - high.astype(F32)
        middle_part = rest.astype(BF16)
        low = (rest - middle_part.astype(F32)).astype(BF16)
        cumulative = dot(ones, high) + (dot(ones, middle_part) + dot(ones, low))
        middle = cumulative[BLOCK // 2 : BLOCK // 2 + 1, :]
        total = cumulative[BLOCK - 1 : BLOCK, :]
        left = query * jnp.exp(cumulative - middle)
        right = gate * jnp.exp(middle - cumulative)
        entering = query * jnp.exp(cumulative)
        leaving = gate * jnp.exp(total - cumulative)
        carried[here, :] = query * jnp.exp(cumulative + offset[...])
        decay = jnp.exp(total)
        for head in range(heads):
            lanes = slice(head * HEAD_DIM, (head + 1) * HEAD_DIM)
            scores = jnp.where(causal, dot_split(left[:, lanes], right[:, lanes], NT), 0.0)
            score_high, score_low = parts(scores)
            held = state[lanes, :]
            values = value[:, lanes]
            out[here, lanes] = dot_split(entering[:, lanes], held, NT) + (
                dot(score_high, values) + dot(score_low, values)
            )
            leave_high, leave_low = parts(leaving[:, lanes])
            state[lanes, :] = decay[:, lanes] * held + (
                dot(values, leave_high, TN) + dot(values, leave_low, TN)
            )
        offset[...] += total
        return 0

    lax.fori_loop(0, rows // BLOCK, step, 0, unroll=2)
    message[0:width, :] = state[...].astype(BF16)
    final = jnp.exp(offset[...])
    tail = jnp.concatenate(
        [final[:, h * HEAD_DIM : (h + 1) * HEAD_DIM] for h in range(heads)]
        + [jnp.zeros((16 - heads, HEAD_DIM), F32)],
        axis=0,
    )
    message[width : width + 16, :] = tail.astype(BF16)


def local_scan(probe, retention, content, slack, surge):
    rows, width = probe.shape
    return pl.pallas_call(
        scan_kernel,
        out_shape=(
            jax.ShapeDtypeStruct((rows, width), F32),
            jax.ShapeDtypeStruct((rows, width), F32),
            jax.ShapeDtypeStruct((width + 16, HEAD_DIM), BF16),
        ),
        in_specs=[VMEM] * 5,
        out_specs=(VMEM, VMEM, VMEM),
        scratch_shapes=[pltpu.VMEM((width, HEAD_DIM), F32), pltpu.VMEM((1, width), F32)],
        name="local_scan",
    )(probe, retention, content, slack.reshape(1, width), surge)


def mix_kernel(order, out, carried, state, emission, gain, *pieces):
    for head in range(out.shape[1] // HEAD_DIM):
        lanes = slice(head * HEAD_DIM, (head + 1) * HEAD_DIM)
        whole = out[:, lanes] + dot_split(carried[:, lanes], state[lanes, :], NT)
        squares = jnp.mean(whole * whole, axis=-1, keepdims=True)
        before = emission[:, lanes].astype(F32)
        scaled = whole * lax.rsqrt(squares + EPSILON) * gain[:, lanes]
        mixed = (scaled * (before * jax.nn.sigmoid(before))).astype(BF16)
        for index, piece in enumerate(pieces):

            @pl.when(pl.program_id(0) == index)
            def _(piece=piece):
                piece[:, lanes] = mixed


def mix(out, carried, state, emission, gain, order):
    rows, width = out.shape
    count = order.shape[0]
    tile = rows // count
    row_spec = pl.BlockSpec((tile, width), lambda i, o: (o[i], 0))
    return pl.pallas_call(
        mix_kernel,
        grid_spec=pltpu.PrefetchScalarGridSpec(
            num_scalar_prefetch=1,
            grid=(count,),
            in_specs=[
                row_spec,
                row_spec,
                pl.BlockSpec((width, HEAD_DIM), lambda i, o: (0, 0)),
                row_spec,
                pl.BlockSpec((1, width), lambda i, o: (0, 0)),
            ],
            out_specs=[pl.BlockSpec((tile, width), lambda i, o: (0, 0))] * count,
        ),
        out_shape=[jax.ShapeDtypeStruct((tile, width), BF16)] * count,
        name="mix",
    )(order, out, carried, state, emission, gain.reshape(1, width))


def project_kernel(count, order, *refs):
    mixed, (weight, skip, gain, stream, normed) = refs[:count], refs[count:]
    width = mixed[0].shape[1]
    total = None
    for index in range(count):
        rows = pl.ds(pl.multiple_of(order[index] * width, width), width)
        term = dot(mixed[index][...], weight[rows, :])
        total = term if total is None else total + term
    added = (skip[...].astype(F32) + total).astype(BF16)
    stream[...] = added
    wide = added.astype(F32)
    squares = jnp.mean(wide * wide, axis=-1, keepdims=True)
    normed[...] = (wide * lax.rsqrt(squares + EPSILON) * gain[...]).astype(BF16)


def project(mixed, order, weight, skip, gain):
    count = len(mixed)
    shape = jax.ShapeDtypeStruct(skip.shape, BF16)
    return pl.pallas_call(
        functools.partial(project_kernel, count),
        in_specs=[pl.BlockSpec(memory_space=pltpu.SMEM)] + [VMEM] * (count + 3),
        out_specs=(VMEM, VMEM),
        out_shape=(shape, shape),
        name="project",
    )(order, *mixed, weight, skip, gain.reshape(1, -1))


def arrivals(length, line):
    below = [(steps, 0) for steps in range(1, line + 1)]
    above = [(steps, 1) for steps in range(1, length - line)]
    return [(0, 0)] + sorted(below + above)


def place_of(length, line, slot):
    result = 0
    for here in range(length):
        steps, side = arrivals(length, here)[slot]
        result = jnp.where(line == here, here + steps if side else here - steps, result)
    return result


def sources(length, slots):
    return [sorted({arrivals(length, here)[slot] for here in range(length)}) for slot in slots]


def pack_kernel(length, slots, matrices, *refs):
    line = lax.axis_index("so")
    packed, sems = refs[-2:]
    names = sources(length, slots)
    cursor = 0
    waits = []
    for matrix in range(matrices):
        for index, slot in enumerate(slots):
            target = packed.at[matrix * len(slots) + index]
            sem = sems.at[matrix * len(slots) + index]
            for name in names[index]:
                source = refs[cursor]
                cursor += 1
                chosen = functools.reduce(
                    jnp.logical_or,
                    [line == i for i in range(length) if arrivals(length, i)[slot] == name],
                )

                @pl.when(chosen)
                def _(source=source, target=target, sem=sem):
                    pltpu.make_async_copy(source, target, sem).start()

            waits.append((source, target, sem))
    for source, target, sem in waits:
        pltpu.make_async_copy(source, target, sem).wait()


def pack(chains, slots, length):
    blocks = [
        chain[name] for chain in chains for names in sources(length, slots) for name in names
    ]
    count = len(chains) * len(slots)
    return pl.pallas_call(
        functools.partial(pack_kernel, length, slots, len(chains)),
        out_shape=jax.ShapeDtypeStruct((count,) + blocks[0].shape, BF16),
        in_specs=[ANY] * len(blocks),
        out_specs=VMEM,
        scratch_shapes=[pltpu.SemaphoreType.DMA((count,))],
        name="pack",
    )(*blocks)


def hidden_kernel(length, groups, count, *refs):
    normed, refs = refs[:count], refs[count:]
    mine, twins = refs[: len(groups)], refs[len(groups) : 2 * len(groups)]
    hidden, rows_now, gate_all, up_all, sems = refs[2 * len(groups) :]
    depth = mine[0].shape[1]
    line = lax.axis_index("so")
    core = lax.axis_index("ti")

    @pl.when(pl.program_id(0) == 0)
    def _():
        copies = []
        for twin, packs in enumerate((mine, twins)):
            side = 1 - core if twin else core
            for pack_ref, slots in zip(packs, groups):
                for matrix, target in enumerate((gate_all, up_all)):
                    for index, slot in enumerate(slots):
                        row = (2 * place_of(length, line, slot) + side) * depth
                        copies.append(
                            pltpu.make_async_copy(
                                pack_ref.at[matrix * len(slots) + index],
                                target.at[pl.ds(pl.multiple_of(row, depth), depth), :],
                                sems.at[(2 * twin + matrix) * length + slot],
                            )
                        )
        for copy in copies:
            copy.start()
        for copy in copies:
            copy.wait()

    for index, piece in enumerate(normed):

        @pl.when(pl.program_id(0) == index)
        def _(piece=piece):
            rows_now[...] = piece[...]

    units = hidden.shape[2]
    for start in range(0, units, CHUNK):
        lanes = slice(start, min(start + CHUNK, units))
        gate = dot(rows_now[...], gate_all[:, lanes])
        up = dot(rows_now[...], up_all[:, lanes])
        hidden[0, :, lanes] = (gate * jax.nn.sigmoid(gate) * up).astype(BF16)


def make_hidden(normed, mine, twins, groups, length):
    rows, features = normed[0].shape
    units = mine[0].shape[2]
    count = len(normed)
    return pl.pallas_call(
        functools.partial(hidden_kernel, length, groups, count),
        grid=(count,),
        out_shape=jax.ShapeDtypeStruct((count, rows, units), BF16),
        in_specs=[pl.BlockSpec((rows, features), lambda i: (0, 0))] * count
        + [ANY] * (2 * len(groups)),
        out_specs=pl.BlockSpec((1, rows, units), lambda i: (i, 0, 0)),
        scratch_shapes=[
            pltpu.VMEM((rows, features), BF16),
            pltpu.VMEM((features, units), BF16),
            pltpu.VMEM((features, units), BF16),
            pltpu.SemaphoreType.DMA((4 * length,)),
        ],
        compiler_params=pltpu.CompilerParams(vmem_limit_bytes=56 * 1024 * 1024),
        name="make_hidden",
    )(*normed, *mine, *twins)


def down_kernel(count, hidden, mine, twins, *refs):
    outs, (weight, sems) = refs[:count], refs[count:]
    slots, columns = mine.shape[0], mine.shape[2]
    copies = []
    for twin, blocks in enumerate((mine, twins)):
        for slot in range(slots):
            target = weight.at[:, pl.ds((2 * slot + twin) * columns, columns)]
            copies.append(
                pltpu.make_async_copy(blocks.at[slot], target, sems.at[2 * slot + twin])
            )
    for copy in copies:
        copy.start()
    for copy in copies:
        copy.wait()
    for index in range(count):
        outs[index][...] = dot(hidden[index], weight[...]).astype(BF16)


def down(hidden, mine, twins):
    count, rows, units = hidden.shape
    width = 2 * mine.shape[0] * mine.shape[2]
    return pl.pallas_call(
        functools.partial(down_kernel, count),
        out_shape=[jax.ShapeDtypeStruct((rows, width), BF16)] * count,
        in_specs=[VMEM, ANY, ANY],
        out_specs=[VMEM] * count,
        scratch_shapes=[
            pltpu.VMEM((units, width), BF16),
            pltpu.SemaphoreType.DMA((2 * mine.shape[0],)),
        ],
        name="down",
    )(hidden, mine, twins)


def finish_kernel(length, groups, count, stream, *refs):
    pieces, out = refs[:-1], refs[-1]
    columns = stream.shape[1] // (2 * length)
    line = lax.axis_index("so")
    side = lax.axis_index("si")
    for group, slots in enumerate(groups):
        mine = pieces[group * count : (group + 1) * count]
        for index, slot in enumerate(slots):
            for twin in range(2):
                block = 2 * place_of(length, line, slot) + (1 - side if twin else side)
                lanes = pl.ds(pl.multiple_of(block * columns, columns), columns)
                start = (2 * index + twin) * columns
                local = slice(start, start + columns)
                total = mine[0][:, local].astype(F32)
                for piece in mine[1:]:
                    total = total + piece[:, local].astype(F32)
                out[:, lanes] = (stream[:, lanes].astype(F32) + total).astype(BF16)


def finish(stream, pieces, groups, length, count):
    return pl.pallas_call(
        functools.partial(finish_kernel, length, groups, count),
        out_shape=jax.ShapeDtypeStruct(stream.shape, BF16),
        in_specs=[VMEM] * (1 + len(pieces)),
        out_specs=VMEM,
        name="finish",
    )(stream, *pieces)


def on_device(
    length,
    ring,
    skip_stream_vector,
    probe_preactivation,
    retention_preactivation,
    content_vector,
    emission_preactivation,
    retention_slack,
    surge_rate,
    subspace_scaling_factor,
    emission_matrix,
    mlp_scaling_factor,
    switch_matrix,
    expansion_matrix,
    contraction_matrix,
):
    width = probe_preactivation.shape[1]
    heads = width // HEAD_DIM
    side = lax.axis_index("si")
    cross = lax.axis_index("to")
    core = lax.axis_index("ti")
    shifts = [(dx, dy) for dx in range(ring) for dy in range(2)]
    up_groups, down_groups = groups_of(length)

    def swapped(a):
        pairs = [(2 * y + c, 2 * c + y) for y in range(2) for c in range(2)]
        return lax.ppermute(a, ("si", "ti"), pairs)

    def traded(a, dx, dy):
        pairs = [
            ((y * ring + x) * 2 + c, ((c ^ dy) * ring + (x + dx) % ring) * 2 + y)
            for y in range(2)
            for x in range(ring)
            for c in range(2)
        ]
        return lax.ppermute(a, ("si", "to", "ti"), pairs)

    def returned(a, dx, dy):
        pairs = [
            (((c ^ dy) * ring + (x + dx) % ring) * 2 + y, (y * ring + x) * 2 + c)
            for y in range(2)
            for x in range(ring)
            for c in range(2)
        ]
        return lax.ppermute(a, ("si", "to", "ti"), pairs)

    def dealt(a, dx, dc):
        pairs = [
            (2 * x + c, 2 * ((x + dx) % ring) + (c ^ dc)) for x in range(ring) for c in range(2)
        ]
        return lax.ppermute(a, ("to", "ti"), pairs)

    def twin(a):
        return lax.ppermute(a, "ti", [(0, 1), (1, 0)])

    def spread(a, direct=False):
        chain = {(0, 0): a}
        lower = upper = a
        for k in range(1, length):
            hop = k if direct else 1
            source = (a, a) if direct else (lower, upper)
            pairs = [(i, i + hop) for i in range(k - hop, length - hop)]
            lower = chain[k, 0] = lax.ppermute(source[0], "so", pairs)
            pairs = [(i + hop, i) for i in range(0, length - k)]
            upper = chain[k, 1] = lax.ppermute(source[1], "so", pairs)
        return chain

    gates = spread(swapped(switch_matrix))
    ups = spread(swapped(expansion_matrix))
    downs = spread(swapped(contraction_matrix), direct=True)

    out, carried, message = local_scan(
        probe_preactivation,
        retention_preactivation,
        content_vector,
        retention_slack,
        surge_rate,
    )

    def opened(a):
        a = a.astype(F32)
        return a[:width].reshape(heads, HEAD_DIM, HEAD_DIM), a[width : width + heads][:, None, :]

    def closed(state, decay):
        return jnp.concatenate(
            [
                state.reshape(width, HEAD_DIM),
                decay.reshape(heads, HEAD_DIM),
                jnp.zeros((16 - heads, HEAD_DIM), F32),
            ]
        ).astype(BF16)

    other = lax.ppermute(message, "si", [(0, 1), (1, 0)])
    first_state, first_decay = opened(jnp.where(side == 0, message, other))
    second_state, second_decay = opened(jnp.where(side == 0, other, message))
    plane = closed(second_decay * first_state + second_state, first_decay * second_decay)
    incoming = jnp.zeros_like(first_state)
    weight = jnp.ones_like(first_decay)
    for k in range(1, length):
        pairs = [(i, i + k) for i in range(length - k)]
        state, decay = opened(lax.ppermute(plane, "so", pairs))
        incoming = incoming + weight * state
        weight = weight * decay
    incoming = jnp.where(side == 0, incoming, first_decay * incoming + first_state)
    came = [lax.rem(cross - dx + ring, ring) * 2 + (core ^ dc) for dx, dc in shifts]
    goes = [lax.rem(cross + dx, ring) * 2 + (core ^ dc) for dx, dc in shifts]
    mixed = mix(
        out,
        carried,
        incoming.reshape(width, HEAD_DIM),
        emission_preactivation,
        subspace_scaling_factor,
        jnp.stack(goes).astype(jnp.int32),
    )
    mixed = [mixed[0]] + [dealt(mixed[index], *shifts[index]) for index in range(1, len(shifts))]
    stream, normed = project(
        mixed,
        jnp.stack(came).astype(jnp.int32),
        emission_matrix,
        skip_stream_vector,
        mlp_scaling_factor,
    )
    normed = [traded(normed, dx, dy) for dx, dy in shifts]

    packs, pack_twins = [], []
    for slots in up_groups:
        packs.append(pack((gates, ups), slots, length))
        pack_twins.append(twin(packs[-1]))
    hidden = make_hidden(normed, packs, pack_twins, up_groups, length)

    pieces = []
    for slots in down_groups:
        mine = pack((downs,), slots, length)
        both = twin(mine)
        parts_out = down(hidden, mine, both)
        for index, (dx, dy) in enumerate(shifts):
            pieces.append(returned(parts_out[index], dx, dy))
    return finish(stream, pieces, down_groups, length, len(shifts))


def groups_of(length):
    last = length - 1
    return (
        (tuple(range(last)), (last,)),
        (tuple(range(last - 1)), (last - 1, last)),
    )


def solution(mesh):
    length, ring = mesh.shape["sp"] // 2, mesh.shape["tp"] // 2
    split = Mesh(mesh.devices.reshape(length, 2, ring, 2), ("so", "si", "to", "ti"))
    sp, tp = ("so", "si"), ("to", "ti")
    in_specs = (
        P(sp + tp, None),
        P(sp, tp),
        P(sp, tp),
        P(sp, tp),
        P(sp, tp),
        P(tp),
        P(sp, tp),
        P(tp),
        P(),
        P(),
        P(sp, tp),
        P(sp, tp),
        P(tp, sp),
    )


    def body(*arguments):
        return on_device(length, ring, *arguments)

    return jax.shard_map(
        body, mesh=split, in_specs=in_specs, out_specs=P(sp + tp, None), check_vma=False
    )
```

profile of v0, /device:TPU:0, one launch (start us, length us, event | category | flops | bytes accessed | tf_op | source)
XLA Modules:
  0.0 340.5 jit_solution(11380273713797615229)
XLA Ops:
  0.0 6.8 %collective-permute-start.11 = (bf16[256,1408]{1,0:T(8,128)(2,1)}, bf16[256,1408]{1,0:T(8,128)(2,1)}, u32[]{:S(2)}, u32[]{:S(2)}) collective-permute-start(bf16[256,1408]{1,0:T(8,128)(2,1)} %param.23), channel_id=1, source_target_pairs={{0,0},{1,4},{4,1},{5,5},{2,2},{3,6},{6,3},{7,7},{8,8},{9,12},{12,9... | collective-permute-start | bytes 2162696 | tf_op jit(solution)/shard_map/ppermute | solution.py:396
  6.8 6.8 %collective-permute-start.16 = (bf16[256,1408]{1,0:T(8,128)(2,1)}, bf16[256,1408]{1,0:T(8,128)(2,1)}, u32[]{:S(2)}, u32[]{:S(2)}) collective-permute-start(bf16[256,1408]{1,0:T(8,128)(2,1)} %param.24), channel_id=1, source_target_pairs={{0,0},{1,4},{4,1},{5,5},{2,2},{3,6},{6,3},{7,7},{8,8},{9,12},{12,9... | collective-permute-start | bytes 2162696 | tf_op jit(solution)/shard_map/ppermute | solution.py:396
  13.7 5.9 %collective-permute-start.12 = (bf16[256,1408]{1,0:T(8,128)(2,1)}, bf16[256,1408]{1,0:T(8,128)(2,1)}, u32[]{:S(2)}, u32[]{:S(2)}) collective-permute-start(bf16[256,1408]{1,0:T(8,128)(2,1)} %collective-permute-done.11.refs_0_), channel_id=1, source_target_pairs={{0,8},{8,16},{16,24},{1,9},{9,17},{17,25},{2,10},{10,18},{18,26},{... | collective-permute-start | bytes 2162696 | tf_op jit(solution)/shard_map/ppermute | solution.py:432
  20.9 5.4 %collective-permute-start.17 = (bf16[256,1408]{1,0:T(8,128)(2,1)}, bf16[256,1408]{1,0:T(8,128)(2,1)}, u32[]{:S(2)}, u32[]{:S(2)}) collective-permute-start(bf16[256,1408]{1,0:T(8,128)(2,1)} %collective-permute-done.16.refs_6_), channel_id=1, source_target_pairs={{0,8},{8,16},{16,24},{1,9},{9,17},{17,25},{2,10},{10,18},{18,26},{... | collective-permute-start | bytes 2162696 | tf_op jit(solution)/shard_map/ppermute | solution.py:432
  27.6 10.9 %local_scan.1 = (f32[1024,256]{1,0:T(8,128)}, f32[1024,256]{1,0:T(8,128)}, bf16[272,128]{1,0:T(8,128)(2,1)}) custom-call(bf16[1024,256]{1,0:T(8,128)(2,1)} %probe.1, bf16[1024,256]{1,0:T(8,128)(2,1)} %retention.1, bf16[1024,256]{1,0:T(8,128)(2,1)} %content.1, f32[1,256]{1,0:T(1,128)} %bitcast.26, f32[1024,256]{1,0:T(8,128)} %surge.1), custom_call_target="tpu_custom_call" | custom-call | tf_op jit(solution)/shard_map/local_scan/pallas_call | solution.py:101
  50.6 5.5 %collective-permute-done.18.refs_8_.refs_9_ = bf16[256,1408]{1,0:T(8,128)(2,1)S(1)} collective-permute-done((bf16[256,1408]{1,0:T(8,128)(2,1)}, bf16[256,1408]{1,0:T(8,128)(2,1)S(1)}, u32[]{:S(2)}, u32[]{:S(2)}) %collective-permute-start.18) | collective-permute-done | bytes 720928 | tf_op jit(solution)/shard_map/ppermute | solution.py:434
  57.5 6.5 %collective-permute-start.2 = (bf16[272,128]{1,0:T(8,128)(2,1)S(1)}, bf16[272,128]{1,0:T(8,128)(2,1)S(1)}, u32[]{:S(2)}, u32[]{:S(2)}) collective-permute-start(bf16[272,128]{1,0:T(8,128)(2,1)S(1)} %maximum_maximum_fusion), channel_id=1, source_target_pairs={{0,16},{8,24},{1,17},{9,25},{2,18},{10,26},{3,19},{11,27},{4,20},{... | collective-permute-start | bytes 208904 | tf_op jit(solution)/shard_map/ppermute | solution.py:470
  66.0 20.3 %collective-permute-start.1 = (bf16[272,128]{1,0:T(8,128)(2,1)S(1)}, bf16[272,128]{1,0:T(8,128)(2,1)S(1)}, u32[]{:S(2)}, u32[]{:S(2)}) collective-permute-start(bf16[272,128]{1,0:T(8,128)(2,1)S(1)} %maximum_maximum_fusion), channel_id=1, source_target_pairs={{0,8},{8,16},{16,24},{1,9},{9,17},{17,25},{2,10},{10,18},{18,26},{... | collective-permute-start | bytes 208904 | tf_op jit(solution)/shard_map/ppermute | solution.py:470
  88.3 7.1 %collective-permute-start.3 = (bf16[272,128]{1,0:T(8,128)(2,1)S(1)}, bf16[272,128]{1,0:T(8,128)(2,1)S(1)}, u32[]{:S(2)}, u32[]{:S(2)}) collective-permute-start(bf16[272,128]{1,0:T(8,128)(2,1)S(1)} %maximum_maximum_fusion), channel_id=1, source_target_pairs={{0,24},{1,25},{2,26},{3,27},{4,28},{5,29},{6,30},{7,31}} | collective-permute-start | bytes 208904 | tf_op jit(solution)/shard_map/ppermute | solution.py:470
  98.0 6.1 %mix.1 = (bf16[256,256]{1,0:T(8,128)(2,1)}, bf16[256,256]{1,0:T(8,128)(2,1)}, bf16[256,256]{1,0:T(8,128)(2,1)}, bf16[256,256]{1,0:T(8,128)(2,1)}) custom-call(s32[4]{0:T(128)} %add_add_fusion.1.order, f32[1024,256]{1,0:T(8,128)} %get-tuple-element.22.out, f32[1024,256]{1,0:T(8,128)} %get-tuple-element.23.carried, f32[256,128]{1,0:T(8,128)} %fusion.4.state, ...), custom_call_target="tpu_custom_call" | custom-call | tf_op jit(solution)/shard_map/mix/pallas_call | solution.py:135
  107.6 4.2 %pack.4.refs_4_ = bf16[6,256,1408]{2,1,0:T(8,128)(2,1)} custom-call(bf16[256,1408]{1,0:T(8,128)(2,1)} %collective-permute-done.11.refs_0_, bf16[256,1408]{1,0:T(8,128)(2,1)} %collective-permute-done.12.refs_1_, bf16[256,1408]{1,0:T(8,128)(2,1)} %copy-done.5, bf16[256,1408]{1,0:T(8,128)(2,1)} %copy-done.5, bf16[256,1408]{1,0:T(8,128)(2,1)} %copy-done.3, ...), custom_call_target="tpu_custom_call" | custom-call | tf_op jit(solution)/shard_map/pack/pallas_call | solution.py:231
  116.1 5.4 %project.1 = (bf16[256,2048]{1,0:T(8,128)(2,1)}, bf16[256,2048]{1,0:T(8,128)(2,1)}) custom-call(s32[4]{0:T(128)} %add_add_fusion.order, bf16[256,256]{1,0:T(8,128)(2,1)} %get-tuple-element.25.refs_0_, bf16[256,256]{1,0:T(8,128)(2,1)} %copy-done.19, bf16[256,256]{1,0:T(8,128)(2,1)} %copy-done.20, bf16[256,256]{1,0:T(8,128)(2,1)} %copy-done.21, ...), custom_call_target="tpu_custom_call" | custom-call | tf_op jit(solution)/shard_map/project/pallas_call | solution.py:172
  127.7 7.9 %collective-permute-start.35 = (bf16[1408,256]{1,0:T(8,128)(2,1)}, bf16[1408,256]{1,0:T(8,128)(2,1)S(1)}, u32[]{:S(2)}, u32[]{:S(2)}) collective-permute-start(bf16[1408,256]{1,0:T(8,128)(2,1)} %collective-permute-done.27.refs_0_), channel_id=1, source_target_pairs={{0,16},{8,24},{1,17},{9,25},{2,18},{10,26},{3,19},{11,27},{4,20},{... | collective-permute-start | bytes 2162696 | tf_op jit(solution)/shard_map/ppermute | solution.py:432
  135.6 11.0 %collective-permute-done.8.refs_1_ = bf16[256,2048]{1,0:T(8,128)(2,1)S(1)} collective-permute-done((bf16[256,2048]{1,0:T(8,128)(2,1)}, bf16[256,2048]{1,0:T(8,128)(2,1)S(1)}, u32[]{:S(2)}, u32[]{:S(2)}) %collective-permute-start.8) | collective-permute-done | bytes 1048608 | tf_op jit(solution)/shard_map/ppermute | solution.py:405
  153.5 10.3 %collective-permute-done.22.refs_3_ = bf16[256,1408]{1,0:T(8,128)(2,1)S(1)} collective-permute-done((bf16[256,1408]{1,0:T(8,128)(2,1)}, bf16[256,1408]{1,0:T(8,128)(2,1)S(1)}, u32[]{:S(2)}, u32[]{:S(2)}) %collective-permute-start.22) | collective-permute-done | bytes 720928 | tf_op jit(solution)/shard_map/ppermute | solution.py:434
  164.7 19.5 %collective-permute-start.37 = (bf16[1408,256]{1,0:T(8,128)(2,1)}, bf16[1408,256]{1,0:T(8,128)(2,1)}, u32[]{:S(2)}, u32[]{:S(2)}) collective-permute-start(bf16[1408,256]{1,0:T(8,128)(2,1)} %collective-permute-done.27.refs_0_), channel_id=1, source_target_pairs={{0,24},{1,25},{2,26},{3,27},{4,28},{5,29},{6,30},{7,31}} | collective-permute-start | bytes 2162696 | tf_op jit(solution)/shard_map/ppermute | solution.py:432
  189.5 19.6 %collective-permute-done.36.refs_2_.refs_4_ = bf16[1408,256]{1,0:T(8,128)(2,1)S(1)} collective-permute-done((bf16[1408,256]{1,0:T(8,128)(2,1)}, bf16[1408,256]{1,0:T(8,128)(2,1)S(1)}, u32[]{:S(2)}, u32[]{:S(2)}) %collective-permute-start.36) | collective-permute-done | bytes 720928 | tf_op jit(solution)/shard_map/ppermute | solution.py:434
  213.8 15.4 %collective-permute-done.38.refs_6_ = bf16[1408,256]{1,0:T(8,128)(2,1)} collective-permute-done((bf16[1408,256]{1,0:T(8,128)(2,1)}, bf16[1408,256]{1,0:T(8,128)(2,1)}, u32[]{:S(2)}, u32[]{:S(2)}) %collective-permute-start.38) | collective-permute-done | bytes 720928 | tf_op jit(solution)/shard_map/ppermute | solution.py:434
  232.5 22.0 %collective-permute-done.10.refs_3_ = bf16[256,2048]{1,0:T(8,128)(2,1)} collective-permute-done((bf16[256,2048]{1,0:T(8,128)(2,1)}, bf16[256,2048]{1,0:T(8,128)(2,1)}, u32[]{:S(2)}, u32[]{:S(2)}) %collective-permute-start.10) | collective-permute-done | bytes 1048608 | tf_op jit(solution)/shard_map/ppermute | solution.py:405
  254.5 21.7 %make_hidden.1.hidden = bf16[4,256,1408]{2,1,0:T(8,128)(2,1)} custom-call(bf16[256,2048]{1,0:T(8,128)(2,1)} %copy-done.9, bf16[256,2048]{1,0:T(8,128)(2,1)} %copy-done.10, bf16[256,2048]{1,0:T(8,128)(2,1)} %collective-permute-done.9.refs_2_, bf16[256,2048]{1,0:T(8,128)(2,1)} %collective-permute-done.10.refs_3_, bf16[6,256,1408]{2,1,0:T(8,128)(2,1)} %pack.4.refs_4_, ...), custom_call_target="tpu_custom_call" | custom-call | tf_op jit(solution)/shard_map/make_hidden/pallas_call | solution.py:288
  277.3 7.8 %down.2 = (bf16[256,1024]{1,0:T(8,128)(2,1)}, bf16[256,1024]{1,0:T(8,128)(2,1)}, bf16[256,1024]{1,0:T(8,128)(2,1)}, bf16[256,1024]{1,0:T(8,128)(2,1)}) custom-call(bf16[4,256,1408]{2,1,0:T(8,128)(2,1)} %make_hidden.1.hidden, bf16[2,1408,256]{2,1,0:T(8,128)(2,1)} %pack.6.mine, bf16[2,1408,256]{2,1,0:T(8,128)(2,1)} %copy-done.8), custom_call_target="tpu_custom_call" | custom-call | tf_op jit(solution)/shard_map/down/pallas_call | solution.py:327
  291.3 7.8 %down.3 = (bf16[256,1024]{1,0:T(8,128)(2,1)}, bf16[256,1024]{1,0:T(8,128)(2,1)}, bf16[256,1024]{1,0:T(8,128)(2,1)}, bf16[256,1024]{1,0:T(8,128)(2,1)}) custom-call(bf16[4,256,1408]{2,1,0:T(8,128)(2,1)} %make_hidden.1.hidden, bf16[2,1408,256]{2,1,0:T(8,128)(2,1)} %pack.7.mine, bf16[2,1408,256]{2,1,0:T(8,128)(2,1)} %copy-done.7), custom_call_target="tpu_custom_call" | custom-call | tf_op jit(solution)/shard_map/down/pallas_call | solution.py:327
  302.8 6.7 %collective-permute-done.32.refs_1_ = bf16[256,1024]{1,0:T(8,128)(2,1)S(1)} collective-permute-done((bf16[256,1024]{1,0:T(8,128)(2,1)}, bf16[256,1024]{1,0:T(8,128)(2,1)S(1)}, u32[]{:S(2)}, u32[]{:S(2)}) %collective-permute-start.32) | collective-permute-done | bytes 524320 | tf_op jit(solution)/shard_map/ppermute | solution.py:414
  313.5 19.8 %collective-permute-done.41.refs_5_ = bf16[256,1024]{1,0:T(8,128)(2,1)S(1)} collective-permute-done((bf16[256,1024]{1,0:T(8,128)(2,1)}, bf16[256,1024]{1,0:T(8,128)(2,1)S(1)}, u32[]{:S(2)}, u32[]{:S(2)}) %collective-permute-start.41) | collective-permute-done | bytes 524320 | tf_op jit(solution)/shard_map/ppermute | solution.py:414
  (134 shorter events, 79.4 us)
Async XLA Ops:
  13.7 30.2 %collective-permute-start.12 = (bf16[256,1408]{1,0:T(8,128)(2,1)}, bf16[256,1408]{1,0:T(8,128)(2,1)}, u32[]{:S(2)}, u32[]{:S(2)}) collective-permute-start(bf16[256,1408]{1,0:T(8,128)(2,1)} %collective-permute-done.11.refs_0_), channel_id=1, source_target_pairs={{0,8},{8,16},{16,24},{1,9},{9,17},{17,25},{2,10},{10,18},{18,26},{... | collective-permute-start | bytes 2162696 | tf_op jit(solution)/shard_map/ppermute | solution.py:432
  19.6 25.1 %collective-permute-start.13 = (bf16[256,1408]{1,0:T(8,128)(2,1)}, bf16[256,1408]{1,0:T(8,128)(2,1)S(1)}, u32[]{:S(2)}, u32[]{:S(2)}) collective-permute-start(bf16[256,1408]{1,0:T(8,128)(2,1)} %collective-permute-done.11.refs_0_), channel_id=1, source_target_pairs={{8,0},{16,8},{24,16},{9,1},{17,9},{25,17},{10,2},{18,10},{26,18},{... | collective-permute-start | bytes 2162696 | tf_op jit(solution)/shard_map/ppermute | solution.py:434
  20.9 28.2 %collective-permute-start.17 = (bf16[256,1408]{1,0:T(8,128)(2,1)}, bf16[256,1408]{1,0:T(8,128)(2,1)}, u32[]{:S(2)}, u32[]{:S(2)}) collective-permute-start(bf16[256,1408]{1,0:T(8,128)(2,1)} %collective-permute-done.16.refs_6_), channel_id=1, source_target_pairs={{0,8},{8,16},{16,24},{1,9},{9,17},{17,25},{2,10},{10,18},{18,26},{... | collective-permute-start | bytes 2162696 | tf_op jit(solution)/shard_map/ppermute | solution.py:432
  26.3 29.8 %collective-permute-start.18 = (bf16[256,1408]{1,0:T(8,128)(2,1)}, bf16[256,1408]{1,0:T(8,128)(2,1)S(1)}, u32[]{:S(2)}, u32[]{:S(2)}) collective-permute-start(bf16[256,1408]{1,0:T(8,128)(2,1)} %collective-permute-done.16.refs_6_), channel_id=1, source_target_pairs={{8,0},{16,8},{24,16},{9,1},{17,9},{25,17},{10,2},{18,10},{26,18},{... | collective-permute-start | bytes 2162696 | tf_op jit(solution)/shard_map/ppermute | solution.py:434
  43.9 60.3 %collective-permute-start.14 = (bf16[256,1408]{1,0:T(8,128)(2,1)}, bf16[256,1408]{1,0:T(8,128)(2,1)S(1)}, u32[]{:S(2)}, u32[]{:S(2)}) collective-permute-start(bf16[256,1408]{1,0:T(8,128)(2,1)} %collective-permute-done.12.refs_1_), channel_id=1, source_target_pairs={{8,16},{16,24},{9,17},{17,25},{10,18},{18,26},{11,19},{19,27},{12,... | collective-permute-start | bytes 2162696 | tf_op jit(solution)/shard_map/ppermute | solution.py:432
  44.6 61.1 %collective-permute-start.15 = (bf16[256,1408]{1,0:T(8,128)(2,1)S(1)}, bf16[256,1408]{1,0:T(8,128)(2,1)}, u32[]{:S(2)}, u32[]{:S(2)}) collective-permute-start(bf16[256,1408]{1,0:T(8,128)(2,1)S(1)} %collective-permute-done.13.refs_2_.refs_3_), channel_id=1, source_target_pairs={{8,0},{16,8},{9,1},{17,9},{10,2},{18,10},{11,3},{19,11},{12,4},{20... | collective-permute-start | bytes 2162696 | tf_op jit(solution)/shard_map/ppermute | solution.py:434
  49.1 57.0 %collective-permute-start.19 = (bf16[256,1408]{1,0:T(8,128)(2,1)}, bf16[256,1408]{1,0:T(8,128)(2,1)}, u32[]{:S(2)}, u32[]{:S(2)}) collective-permute-start(bf16[256,1408]{1,0:T(8,128)(2,1)} %collective-permute-done.17.refs_7_), channel_id=1, source_target_pairs={{8,16},{16,24},{9,17},{17,25},{10,18},{18,26},{11,19},{19,27},{12,... | collective-permute-start | bytes 2162696 | tf_op jit(solution)/shard_map/ppermute | solution.py:432
  56.1 51.5 %collective-permute-start.20 = (bf16[256,1408]{1,0:T(8,128)(2,1)S(1)}, bf16[256,1408]{1,0:T(8,128)(2,1)}, u32[]{:S(2)}, u32[]{:S(2)}) collective-permute-start(bf16[256,1408]{1,0:T(8,128)(2,1)S(1)} %collective-permute-done.18.refs_8_.refs_9_), channel_id=1, source_target_pairs={{8,0},{16,8},{9,1},{17,9},{10,2},{18,10},{11,3},{19,11},{12,4},{20... | collective-permute-start | bytes 2162696 | tf_op jit(solution)/shard_map/ppermute | solution.py:434
  111.9 142.6 %collective-permute-start.25 = (bf16[6,256,1408]{2,1,0:T(8,128)(2,1)}, bf16[6,256,1408]{2,1,0:T(8,128)(2,1)}, u32[]{:S(2)}, u32[]{:S(2)}) collective-permute-start(bf16[6,256,1408]{2,1,0:T(8,128)(2,1)} %pack.4.refs_4_), channel_id=1, source_target_pairs={{0,1},{1,0},{2,3},{3,2},{4,5},{5,4},{6,7},{7,6},{8,9},{9,8},{10,11... | collective-permute-start | bytes 12976136 | tf_op jit(solution)/shard_map/ppermute | solution.py:423
  127.7 23.2 %collective-permute-start.35 = (bf16[1408,256]{1,0:T(8,128)(2,1)}, bf16[1408,256]{1,0:T(8,128)(2,1)S(1)}, u32[]{:S(2)}, u32[]{:S(2)}) collective-permute-start(bf16[1408,256]{1,0:T(8,128)(2,1)} %collective-permute-done.27.refs_0_), channel_id=1, source_target_pairs={{0,16},{8,24},{1,17},{9,25},{2,18},{10,26},{3,19},{11,27},{4,20},{... | collective-permute-start | bytes 2162696 | tf_op jit(solution)/shard_map/ppermute | solution.py:432
  149.4 34.8 %collective-permute-start.23 = (bf16[256,1408]{1,0:T(8,128)(2,1)}, bf16[256,1408]{1,0:T(8,128)(2,1)}, u32[]{:S(2)}, u32[]{:S(2)}) collective-permute-start(bf16[256,1408]{1,0:T(8,128)(2,1)} %collective-permute-done.19.refs_10_.refs_4_), channel_id=1, source_target_pairs={{16,24},{17,25},{18,26},{19,27},{20,28},{21,29},{22,30},{23,31}} | collective-permute-start | bytes 2162696 | tf_op jit(solution)/shard_map/ppermute | solution.py:432
  150.9 34.8 %collective-permute-start.24 = (bf16[256,1408]{1,0:T(8,128)(2,1)}, bf16[256,1408]{1,0:T(8,128)(2,1)}, u32[]{:S(2)}, u32[]{:S(2)}) collective-permute-start(bf16[256,1408]{1,0:T(8,128)(2,1)} %collective-permute-done.20.refs_11_.refs_5_), channel_id=1, source_target_pairs={{8,0},{9,1},{10,2},{11,3},{12,4},{13,5},{14,6},{15,7}} | collective-permute-start | bytes 2162696 | tf_op jit(solution)/shard_map/ppermute | solution.py:434
  152.2 56.9 %collective-permute-start.36 = (bf16[1408,256]{1,0:T(8,128)(2,1)}, bf16[1408,256]{1,0:T(8,128)(2,1)S(1)}, u32[]{:S(2)}, u32[]{:S(2)}) collective-permute-start(bf16[1408,256]{1,0:T(8,128)(2,1)} %collective-permute-done.27.refs_0_), channel_id=1, source_target_pairs={{16,0},{24,8},{17,1},{25,9},{18,2},{26,10},{19,3},{27,11},{20,4},{... | collective-permute-start | bytes 2162696 | tf_op jit(solution)/shard_map/ppermute | solution.py:434
  164.7 48.8 %collective-permute-start.37 = (bf16[1408,256]{1,0:T(8,128)(2,1)}, bf16[1408,256]{1,0:T(8,128)(2,1)}, u32[]{:S(2)}, u32[]{:S(2)}) collective-permute-start(bf16[1408,256]{1,0:T(8,128)(2,1)} %collective-permute-done.27.refs_0_), channel_id=1, source_target_pairs={{0,24},{1,25},{2,26},{3,27},{4,28},{5,29},{6,30},{7,31}} | collective-permute-start | bytes 2162696 | tf_op jit(solution)/shard_map/ppermute | solution.py:432
  184.2 47.5 %collective-permute-start.9 = (bf16[256,2048]{1,0:T(8,128)(2,1)}, bf16[256,2048]{1,0:T(8,128)(2,1)}, u32[]{:S(2)}, u32[]{:S(2)}) collective-permute-start(bf16[256,2048]{1,0:T(8,128)(2,1)} %get-tuple-element.30), channel_id=1, source_target_pairs={{0,2},{1,6},{2,0},{3,4},{4,3},{5,7},{6,1},{7,5},{8,10},{9,14},{10,... | collective-permute-start | bytes 3145736 | tf_op jit(solution)/shard_map/ppermute | solution.py:405
  185.7 43.5 %collective-permute-start.38 = (bf16[1408,256]{1,0:T(8,128)(2,1)}, bf16[1408,256]{1,0:T(8,128)(2,1)}, u32[]{:S(2)}, u32[]{:S(2)}) collective-permute-start(bf16[1408,256]{1,0:T(8,128)(2,1)} %collective-permute-done.27.refs_0_), channel_id=1, source_target_pairs={{24,0},{25,1},{26,2},{27,3},{28,4},{29,5},{30,6},{31,7}} | collective-permute-start | bytes 2162696 | tf_op jit(solution)/shard_map/ppermute | solution.py:434
  209.1 45.4 %collective-permute-start.26 = (bf16[2,256,1408]{2,1,0:T(8,128)(2,1)}, bf16[2,256,1408]{2,1,0:T(8,128)(2,1)}, u32[]{:S(2)}, u32[]{:S(2)}) collective-permute-start(bf16[2,256,1408]{2,1,0:T(8,128)(2,1)} %pack.5.refs_5_), channel_id=1, source_target_pairs={{0,1},{1,0},{2,3},{3,2},{4,5},{5,4},{6,7},{7,6},{8,9},{9,8},{10,11... | collective-permute-start | bytes 4325384 | tf_op jit(solution)/shard_map/ppermute | solution.py:423
  213.5 62.7 %collective-permute-start.30 = (bf16[2,1408,256]{2,1,0:T(8,128)(2,1)}, bf16[2,1408,256]{2,1,0:T(8,128)(2,1)S(1)}, u32[]{:S(2)}, u32[]{:S(2)}) collective-permute-start(bf16[2,1408,256]{2,1,0:T(8,128)(2,1)} %pack.6.mine), channel_id=1, source_target_pairs={{0,1},{1,0},{2,3},{3,2},{4,5},{5,4},{6,7},{7,6},{8,9},{9,8},{10,11... | collective-permute-start | bytes 4325384 | tf_op jit(solution)/shard_map/ppermute | solution.py:423
  229.2 25.3 %collective-permute-start.10 = (bf16[256,2048]{1,0:T(8,128)(2,1)}, bf16[256,2048]{1,0:T(8,128)(2,1)}, u32[]{:S(2)}, u32[]{:S(2)}) collective-permute-start(bf16[256,2048]{1,0:T(8,128)(2,1)} %get-tuple-element.30), channel_id=1, source_target_pairs={{0,6},{1,2},{2,4},{3,0},{4,7},{5,3},{6,5},{7,1},{8,14},{9,10},{10,... | collective-permute-start | bytes 3145736 | tf_op jit(solution)/shard_map/ppermute | solution.py:405
  231.7 58.4 %collective-permute-start.39 = (bf16[2,1408,256]{2,1,0:T(8,128)(2,1)}, bf16[2,1408,256]{2,1,0:T(8,128)(2,1)S(1)}, u32[]{:S(2)}, u32[]{:S(2)}) collective-permute-start(bf16[2,1408,256]{2,1,0:T(8,128)(2,1)} %pack.7.mine), channel_id=1, source_target_pairs={{0,1},{1,0},{2,3},{3,2},{4,5},{5,4},{6,7},{7,6},{8,9},{9,8},{10,11... | collective-permute-start | bytes 4325384 | tf_op jit(solution)/shard_map/ppermute | solution.py:423
  289.6 23.9 %collective-permute-start.34 = (bf16[256,1024]{1,0:T(8,128)(2,1)}, bf16[256,1024]{1,0:T(8,128)(2,1)S(1)}, u32[]{:S(2)}, u32[]{:S(2)}) collective-permute-start(bf16[256,1024]{1,0:T(8,128)(2,1)} %get-tuple-element.34), channel_id=1, source_target_pairs={{6,0},{2,1},{4,2},{0,3},{7,4},{3,5},{5,6},{1,7},{14,8},{10,9},{12,... | collective-permute-start | bytes 1572872 | tf_op jit(solution)/shard_map/ppermute | solution.py:414
  300.8 32.5 %collective-permute-start.41 = (bf16[256,1024]{1,0:T(8,128)(2,1)}, bf16[256,1024]{1,0:T(8,128)(2,1)S(1)}, u32[]{:S(2)}, u32[]{:S(2)}) collective-permute-start(bf16[256,1024]{1,0:T(8,128)(2,1)} %get-tuple-element.36), channel_id=1, source_target_pairs={{4,0},{0,1},{6,2},{2,3},{5,4},{1,5},{7,6},{3,7},{12,8},{8,9},{14,1... | collective-permute-start | bytes 1572872 | tf_op jit(solution)/shard_map/ppermute | solution.py:414
  309.5 23.8 %collective-permute-start.42 = (bf16[256,1024]{1,0:T(8,128)(2,1)}, bf16[256,1024]{1,0:T(8,128)(2,1)}, u32[]{:S(2)}, u32[]{:S(2)}) collective-permute-start(bf16[256,1024]{1,0:T(8,128)(2,1)} %get-tuple-element.37), channel_id=1, source_target_pairs={{2,0},{6,1},{0,2},{4,3},{3,4},{7,5},{1,6},{5,7},{10,8},{14,9},{8,1... | collective-permute-start | bytes 1572872 | tf_op jit(solution)/shard_map/ppermute | solution.py:414
  310.9 25.4 %collective-permute-start.43 = (bf16[256,1024]{1,0:T(8,128)(2,1)}, bf16[256,1024]{1,0:T(8,128)(2,1)}, u32[]{:S(2)}, u32[]{:S(2)}) collective-permute-start(bf16[256,1024]{1,0:T(8,128)(2,1)} %get-tuple-element.38), channel_id=1, source_target_pairs={{6,0},{2,1},{4,2},{0,3},{7,4},{3,5},{5,6},{1,7},{14,8},{10,9},{12,... | collective-permute-start | bytes 1572872 | tf_op jit(solution)/shard_map/ppermute | solution.py:414
  (43 other events, 704.8 us)
where the time goes:
time: 342 us; the launch traced here: 340 us
  starting transfers between devices  131 us (38%)
  waiting for transfers between devices  126 us (37%)
  Pallas kernels  75.5 us (22%)
  local copies, waits for them, and re-layouts  4.04 us (1%)
    ppermute x9, waiting for transfers between devices, spread(): upper = chain[k, 1] = lax.ppermute(source[1], 'so', pairs)  50.8 us
    ppermute x9, starting transfers between devices, spread(): lower = chain[k, 0] = lax.ppermute(source[0], 'so', pairs)  45.3 us
    ppermute x3, starting transfers between devices, on_device(): state, decay = opened(lax.ppermute(plane, 'so', pairs))  33.9 us
    ppermute x4, waiting for transfers between devices, traded(): return lax.ppermute(a, ('si', 'to', 'ti'), pairs)  33 us
    ppermute x8, waiting for transfers between devices, returned(): return lax.ppermute(a, ('si', 'to', 'ti'), pairs)  31.2 us
    pallas_call x1, Pallas kernels, make_hidden(): pl.pallas_call(functools.partial(hidden_kernel, length, groups, count), g...  21.7 us
    pallas_call x2, Pallas kernels, down(): pl.pallas_call(functools.partial(down_kernel, count), out_shape=[jax.Shap...  15.7 us
    ppermute x3, starting transfers between devices, swapped(): return lax.ppermute(a, ('si', 'ti'), pairs)  15.2 us
  transfers between devices with their start and end apart: 44, of which 15 were waited for; matrix products, arithmetic and copies ran while one was open for 1% of the time, Pallas kernels for 21%

commit v1 on v0

--- a/solution.py
+++ b/solution.py
@@ -12,6 +12,7 @@
 HEAD_DIM = 128
 BLOCK = 64
 CHUNK = 512
+ROOM = 66_000_000
 EPSILON = 1e-06
 F32 = jnp.float32
 BF16 = jnp.bfloat16
@@ -85,7 +86,7 @@
         offset[...] += total
         return 0
 
-    lax.fori_loop(0, rows // BLOCK, step, 0, unroll=2)
+    lax.fori_loop(0, rows // BLOCK, step, 0, unroll=4)
     message[0:width, :] = state[...].astype(BF16)
     final = jnp.exp(offset[...])
     tail = jnp.concatenate(
@@ -178,163 +179,202 @@
     )(order, *mixed, weight, skip, gain.reshape(1, -1))
 
 
-def arrivals(length, line):
-    below = [(steps, 0) for steps in range(1, line + 1)]
-    above = [(steps, 1) for steps in range(1, length - line)]
-    return [(0, 0)] + sorted(below + above)
-
-
-def place_of(length, line, slot):
-    result = 0
-    for here in range(length):
-        steps, side = arrivals(length, here)[slot]
-        result = jnp.where(line == here, here + steps if side else here - steps, result)
-    return result
-
-
-def sources(length, slots):
-    return [sorted({arrivals(length, here)[slot] for here in range(length)}) for slot in slots]
-
-
-def pack_kernel(length, slots, matrices, *refs):
-    line = lax.axis_index("so")
-    packed, sems = refs[-2:]
-    names = sources(length, slots)
-    cursor = 0
-    waits = []
-    for matrix in range(matrices):
-        for index, slot in enumerate(slots):
-            target = packed.at[matrix * len(slots) + index]
-            sem = sems.at[matrix * len(slots) + index]
-            for name in names[index]:
-                source = refs[cursor]
-                cursor += 1
-                chosen = functools.reduce(
-                    jnp.logical_or,
-                    [line == i for i in range(length) if arrivals(length, i)[slot] == name],
-                )
-
-                @pl.when(chosen)
-                def _(source=source, target=target, sem=sem):
-                    pltpu.make_async_copy(source, target, sem).start()
-
-            waits.append((source, target, sem))
-    for source, target, sem in waits:
-        pltpu.make_async_copy(source, target, sem).wait()
-
-
-def pack(chains, slots, length):
-    blocks = [
-        chain[name] for chain in chains for names in sources(length, slots) for name in names
+def arrivals(length):
+    offsets = [0]
+    for step in range(1, length // 2 + 1):
+        offsets += [step, length - step][: min(2, length - len(offsets))]
+    return offsets
+
+
+def column_place(line, offset, length):
+    return lax.rem(line - offset + length, length)
+
+
+def pack_kernel(*refs):
+    blocks, (packed, sems) = refs[:-2], refs[-2:]
+    copies = [
+        pltpu.make_async_copy(block, packed.at[index], sems.at[index])
+        for index, block in enumerate(blocks)
     ]
-    count = len(chains) * len(slots)
-    return pl.pallas_call(
-        functools.partial(pack_kernel, length, slots, len(chains)),
+    for copy in copies:
+        copy.start()
+    for copy in copies:
+        copy.wait()
+
+
+def pack(blocks):
+    count = len(blocks)
+    return pl.pallas_call(
+        pack_kernel,
         out_shape=jax.ShapeDtypeStruct((count,) + blocks[0].shape, BF16),
-        in_specs=[ANY] * len(blocks),
+        in_specs=[ANY] * count,
         out_specs=VMEM,
         scratch_shapes=[pltpu.SemaphoreType.DMA((count,))],
         name="pack",
     )(*blocks)
 
 
-def hidden_kernel(length, groups, count, *refs):
+def hidden_kernel(length, count, *refs):
     normed, refs = refs[:count], refs[count:]
-    mine, twins = refs[: len(groups)], refs[len(groups) : 2 * len(groups)]
-    hidden, rows_now, gate_all, up_all, sems = refs[2 * len(groups) :]
-    depth = mine[0].shape[1]
+    gates, ups, refs = refs[:length], refs[length : 2 * length], refs[2 * length :]
+    (packed, last_gate, last_up, down_own, down_twin), refs = refs[:5], refs[5:]
+    hidden, outs, refs = refs[0], refs[1 : 1 + count], refs[1 + count :]
+    rows_now, gate_all, up_all, down_all, gate_sum, up_sum, sems, piece_sem = refs
+    depth, units = gates[0].shape
+    columns = down_own.shape[1]
     line = lax.axis_index("so")
     core = lax.axis_index("ti")
-
-    @pl.when(pl.program_id(0) == 0)
+    turn = pl.program_id(0)
+    early = length - 1
+
+    height = normed[0].shape[0]
+    group = hidden.shape[0] // height
+    half = length * depth
+
+    places = []
+    weight_copies = []
+    for twin in range(2):
+        side = 1 - core if twin else core
+        for index, offset in enumerate(arrivals(length)):
+            if not twin:
+                gate_block, up_block = gates[index], ups[index]
+            elif index < early:
+                gate_block, up_block = packed.at[index], packed.at[early + index]
+            else:
+                gate_block, up_block = last_gate, last_up
+            slot = twin * length + index
+            rows = pl.ds(slot * depth, depth)
+            weight_copies += [
+                pltpu.make_async_copy(gate_block, gate_all.at[rows, :], sems.at[2 * slot]),
+                pltpu.make_async_copy(up_block, up_all.at[rows, :], sems.at[2 * slot + 1]),
+            ]
+            places.append(2 * column_place(line, offset, length) + side)
+    down_copies = [
+        pltpu.make_async_copy(
+            block, down_all.at[:, pl.ds(index * columns, columns)], sems.at[4 * length + index]
+        )
+        for index, block in enumerate((down_own, down_twin))
+    ]
+
+    def piece_copies(piece):
+        return [
+            pltpu.make_async_copy(
+                normed[piece].at[:, pl.ds(pl.multiple_of(place * depth, depth), depth)],
+                rows_now.at[pl.ds(piece * height, height), pl.ds(slot * depth, depth)],
+                piece_sem.at[piece * 2 * length + slot],
+            )
+            for slot, place in enumerate(places)
+        ]
+
+    chunks = [slice(start, min(start + CHUNK, units)) for start in range(0, units, CHUNK)]
+
+    @pl.when(turn == 0)
     def _():
-        copies = []
-        for twin, packs in enumerate((mine, twins)):
-            side = 1 - core if twin else core
-            for pack_ref, slots in zip(packs, groups):
-                for matrix, target in enumerate((gate_all, up_all)):
-                    for index, slot in enumerate(slots):
-                        row = (2 * place_of(length, line, slot) + side) * depth
-                        copies.append(
-                            pltpu.make_async_copy(
-                                pack_ref.at[matrix * len(slots) + index],
-                                target.at[pl.ds(pl.multiple_of(row, depth), depth), :],
-                                sems.at[(2 * twin + matrix) * length + slot],
-                            )
-                        )
-        for copy in copies:
+        first = [copy for piece in range(group) for copy in piece_copies(piece)]
+        others = [copy for piece in range(group, count) for copy in piece_copies(piece)]
+        for copy in first + weight_copies + down_copies + others:
             copy.start()
-        for copy in copies:
+        for copy in first + weight_copies[: 2 * length]:
             copy.wait()
-
-    for index, piece in enumerate(normed):
-
-        @pl.when(pl.program_id(0) == index)
+        now = slice(0, group * height)
+        for lanes in chunks:
+            gate_sum[:, lanes] = dot(rows_now[now, :half], gate_all[:half, lanes])
+            up_sum[:, lanes] = dot(rows_now[now, :half], up_all[:half, lanes])
+        for copy in weight_copies[2 * length :]:
+            copy.wait()
+        for lanes in chunks:
+            gate = gate_sum[:, lanes] + dot(rows_now[now, half:], gate_all[half:, lanes])
+            up = up_sum[:, lanes] + dot(rows_now[now, half:], up_all[half:, lanes])
+            hidden[:, lanes] = (gate * jax.nn.sigmoid(gate) * up).astype(BF16)
+        for copy in down_copies:
+            copy.wait()
+
+    for piece in range(group, count):
+
+        @pl.when(turn == piece // group)
         def _(piece=piece):
-            rows_now[...] = piece[...]
-
-    units = hidden.shape[2]
-    for start in range(0, units, CHUNK):
-        lanes = slice(start, min(start + CHUNK, units))
-        gate = dot(rows_now[...], gate_all[:, lanes])
-        up = dot(rows_now[...], up_all[:, lanes])
-        hidden[0, :, lanes] = (gate * jax.nn.sigmoid(gate) * up).astype(BF16)
-
-
-def make_hidden(normed, mine, twins, groups, length):
+            for copy in piece_copies(piece):
+                copy.wait()
+
+    @pl.when(turn > 0)
+    def _():
+        here = pl.ds(pl.multiple_of(turn * group * height, group * height), group * height)
+        for lanes in chunks:
+            gate = dot(rows_now[here, :], gate_all[:, lanes])
+            up = dot(rows_now[here, :], up_all[:, lanes])
+            hidden[:, lanes] = (gate * jax.nn.sigmoid(gate) * up).astype(BF16)
+
+    share = dot(hidden[...], down_all[...]).astype(BF16)
+    for index in range(count):
+
+        @pl.when(turn == index // group)
+        def _(index=index):
+            start = index % group * height
+            outs[index][...] = share[start : start + height, :]
+
+
+def make_hidden(normed, gates, ups, packed, last_gate, last_up, down_own, down_twin):
     rows, features = normed[0].shape
-    units = mine[0].shape[2]
+    length = len(gates)
+    units = gates[0].shape[1]
+    columns = 2 * down_own.shape[1]
     count = len(normed)
     return pl.pallas_call(
-        functools.partial(hidden_kernel, length, groups, count),
-        grid=(count,),
-        out_shape=jax.ShapeDtypeStruct((count, rows, units), BF16),
-        in_specs=[pl.BlockSpec((rows, features), lambda i: (0, 0))] * count
-        + [ANY] * (2 * len(groups)),
-        out_specs=pl.BlockSpec((1, rows, units), lambda i: (i, 0, 0)),
+        functools.partial(hidden_kernel, length, count),
+        grid=(count // 2,),
+        out_shape=[jax.ShapeDtypeStruct((count * rows, units), BF16)]
+        + [jax.ShapeDtypeStruct((rows, columns), BF16)] * count,
+        in_specs=[ANY] * (count + 2 * length + 5),
+        out_specs=[pl.BlockSpec((2 * rows, units), lambda i: (i, 0))]
+        + [pl.BlockSpec((rows, columns), lambda i: (0, 0))] * count,
         scratch_shapes=[
-            pltpu.VMEM((rows, features), BF16),
+            pltpu.VMEM((count * rows, features), BF16),
             pltpu.VMEM((features, units), BF16),
             pltpu.VMEM((features, units), BF16),
-            pltpu.SemaphoreType.DMA((4 * length,)),
+            pltpu.VMEM((units, columns), BF16),
+            pltpu.VMEM((2 * rows, units), F32),
+            pltpu.VMEM((2 * rows, units), F32),
+            pltpu.SemaphoreType.DMA((4 * length + 2,)),
+            pltpu.SemaphoreType.DMA((2 * length * count,)),
         ],
-        compiler_params=pltpu.CompilerParams(vmem_limit_bytes=56 * 1024 * 1024),
+        compiler_params=pltpu.CompilerParams(vmem_limit_bytes=ROOM),
         name="make_hidden",
-    )(*normed, *mine, *twins)
-
-
-def down_kernel(count, hidden, mine, twins, *refs):
-    outs, (weight, sems) = refs[:count], refs[count:]
-    slots, columns = mine.shape[0], mine.shape[2]
-    copies = []
-    for twin, blocks in enumerate((mine, twins)):
-        for slot in range(slots):
-            target = weight.at[:, pl.ds((2 * slot + twin) * columns, columns)]
-            copies.append(
-                pltpu.make_async_copy(blocks.at[slot], target, sems.at[2 * slot + twin])
-            )
+    )(*normed, *gates, *ups, packed, last_gate, last_up, down_own, down_twin)
+
+
+def down_kernel(count, blocks, hidden, *refs):
+    weights, outs, (weight, sems) = refs[:blocks], refs[blocks : blocks + count], refs[-2:]
+    columns = weights[0].shape[1]
+    rows = outs[0].shape[0]
+    copies = [
+        pltpu.make_async_copy(
+            block, weight.at[:, pl.ds(index * columns, columns)], sems.at[index]
+        )
+        for index, block in enumerate(weights)
+    ]
     for copy in copies:
         copy.start()
     for copy in copies:
         copy.wait()
     for index in range(count):
-        outs[index][...] = dot(hidden[index], weight[...]).astype(BF16)
-
-
-def down(hidden, mine, twins):
-    count, rows, units = hidden.shape
-    width = 2 * mine.shape[0] * mine.shape[2]
-    return pl.pallas_call(
-        functools.partial(down_kernel, count),
-        out_shape=[jax.ShapeDtypeStruct((rows, width), BF16)] * count,
-        in_specs=[VMEM, ANY, ANY],
+        here = hidden[index * rows : (index + 1) * rows, :]
+        outs[index][...] = dot(here, weight[...]).astype(BF16)
+
+
+def down(hidden, blocks, count):
+    rows, units = hidden.shape
+    width = len(blocks) * blocks[0].shape[1]
+    return pl.pallas_call(
+        functools.partial(down_kernel, count, len(blocks)),
+        out_shape=[jax.ShapeDtypeStruct((rows // count, width), BF16)] * count,
+        in_specs=[VMEM] + [ANY] * len(blocks),
         out_specs=[VMEM] * count,
         scratch_shapes=[
             pltpu.VMEM((units, width), BF16),
-            pltpu.SemaphoreType.DMA((2 * mine.shape[0],)),
+            pltpu.SemaphoreType.DMA((len(blocks),)),
         ],
         name="down",
-    )(hidden, mine, twins)
+    )(hidden, *blocks)
 
 
 def finish_kernel(length, groups, count, stream, *refs):
@@ -342,11 +382,12 @@
     columns = stream.shape[1] // (2 * length)
     line = lax.axis_index("so")
     side = lax.axis_index("si")
-    for group, slots in enumerate(groups):
+    for group, offsets in enumerate(groups):
         mine = pieces[group * count : (group + 1) * count]
-        for index, slot in enumerate(slots):
+        for index, offset in enumerate(offsets):
             for twin in range(2):
-                block = 2 * place_of(length, line, slot) + (1 - side if twin else side)
+                place = column_place(line, offset, length)
+                block = 2 * place + (1 - side if twin else side)
                 lanes = pl.ds(pl.multiple_of(block * columns, columns), columns)
                 start = (2 * index + twin) * columns
                 local = slice(start, start + columns)
@@ -357,12 +398,67 @@
 
 
 def finish(stream, pieces, groups, length, count):
-    return pl.pallas_call(
-        functools.partial(finish_kernel, length, groups, count),
+    def kernel(stream_ref, *refs):
+        refs[-1][...] = stream_ref[...]
+        finish_kernel(length, groups, count, stream_ref, *refs)
+
+    return pl.pallas_call(
+        kernel,
         out_shape=jax.ShapeDtypeStruct(stream.shape, BF16),
         in_specs=[VMEM] * (1 + len(pieces)),
         out_specs=VMEM,
         name="finish",
+    )(stream, *pieces)
+
+
+def last_kernel(length, offsets, stream, *refs):
+    pieces, (out, held, done, read_sems, write_sems) = refs[:-5], refs[-5:]
+    columns = held.shape[2]
+    line = lax.axis_index("so")
+    side = lax.axis_index("si")
+    moves = []
+    for index, offset in enumerate(offsets):
+        for twin in range(2):
+            block = 2 * column_place(line, offset, length) + (1 - side if twin else side)
+            lanes = pl.ds(pl.multiple_of(block * columns, columns), columns)
+            slot = 2 * index + twin
+            moves.append(
+                (
+                    pltpu.make_async_copy(stream.at[:, lanes], held.at[slot], read_sems.at[slot]),
+                    pltpu.make_async_copy(done.at[slot], out.at[:, lanes], write_sems.at[slot]),
+                )
+            )
+    for read, _ in moves:
+        read.start()
+    for slot, (read, write) in enumerate(moves):
+        local = slice(slot * columns, (slot + 1) * columns)
+        total = pieces[0][:, local].astype(F32)
+        for piece in pieces[1:]:
+            total = total + piece[:, local].astype(F32)
+        read.wait()
+        done[slot] = (held[slot].astype(F32) + total).astype(BF16)
+        write.start()
+    for _, write in moves:
+        write.wait()
+
+
+def finish_last(stream, pieces, offsets, length):
+    rows = stream.shape[0]
+    count = 2 * len(offsets)
+    columns = pieces[0].shape[1] // count
+    return pl.pallas_call(
+        functools.partial(last_kernel, length, offsets),
+        out_shape=jax.ShapeDtypeStruct(stream.shape, BF16),
+        in_specs=[ANY] + [VMEM] * len(pieces),
+        out_specs=ANY,
+        scratch_shapes=[
+            pltpu.VMEM((count, rows, columns), BF16),
+            pltpu.VMEM((count, rows, columns), BF16),
+            pltpu.SemaphoreType.DMA((count,)),
+            pltpu.SemaphoreType.DMA((count,)),
+        ],
+        input_output_aliases={0: 0},
+        name="finish_last",
     )(stream, *pieces)
 
 
@@ -389,7 +485,8 @@
     cross = lax.axis_index("to")
     core = lax.axis_index("ti")
     shifts = [(dx, dy) for dx in range(ring) for dy in range(2)]
-    up_groups, down_groups = groups_of(length)
+    order = arrivals(length)
+    down_groups = groups_of(length)
 
     def swapped(a):
         pairs = [(2 * y + c, 2 * c + y) for y in range(2) for c in range(2)]
@@ -422,21 +519,29 @@
     def twin(a):
         return lax.ppermute(a, "ti", [(0, 1), (1, 0)])
 
-    def spread(a, direct=False):
-        chain = {(0, 0): a}
-        lower = upper = a
-        for k in range(1, length):
-            hop = k if direct else 1
-            source = (a, a) if direct else (lower, upper)
-            pairs = [(i, i + hop) for i in range(k - hop, length - hop)]
-            lower = chain[k, 0] = lax.ppermute(source[0], "so", pairs)
-            pairs = [(i + hop, i) for i in range(0, length - k)]
-            upper = chain[k, 1] = lax.ppermute(source[1], "so", pairs)
-        return chain
-
-    gates = spread(swapped(switch_matrix))
+    def spread(a, held=None):
+        blocks = [a] * length
+        for step in range(1, length // 2 + 1):
+            if step == 1 and held is not None:
+                pairs = [
+                    ((i * 2 + y) * 2 + c, ((i + 1) % length * 2 + c) * 2 + y)
+                    for i in range(length)
+                    for y in range(2)
+                    for c in range(2)
+                ]
+                blocks[step] = lax.ppermute(held, ("so", "si", "ti"), pairs)
+                continue
+            pairs = [(i, (i + 1) % length) for i in range(length)]
+            blocks[step] = lax.ppermute(blocks[step - 1], "so", pairs)
+        for step in range(1, (length - 1) // 2 + 1):
+            pairs = [((i + 1) % length, i) for i in range(length)]
+            source = blocks[(length - step + 1) % length]
+            blocks[length - step] = lax.ppermute(source, "so", pairs)
+        return blocks
+
+    gates = spread(swapped(switch_matrix), switch_matrix)
     ups = spread(swapped(expansion_matrix))
-    downs = spread(swapped(contraction_matrix), direct=True)
+    downs = spread(swapped(contraction_matrix))
 
     out, carried, message = local_scan(
         probe_preactivation,
@@ -491,28 +596,29 @@
     )
     normed = [traded(normed, dx, dy) for dx, dy in shifts]
 
-    packs, pack_twins = [], []
-    for slots in up_groups:
-        packs.append(pack((gates, ups), slots, length))
-        pack_twins.append(twin(packs[-1]))
-    hidden = make_hidden(normed, packs, pack_twins, up_groups, length)
+    gates = [gates[offset] for offset in order]
+    ups = [ups[offset] for offset in order]
+    packed = pack(gates[:-1] + ups[:-1])
+    packed = twin(packed)
+    down_twins = [twin(block) for block in downs]
+    last_twins = twin(gates[-1]), twin(ups[-1])
+    hidden, *first = make_hidden(normed, gates, ups, packed, *last_twins, downs[0], down_twins[0])
 
     pieces = []
-    for slots in down_groups:
-        mine = pack((downs,), slots, length)
-        both = twin(mine)
-        parts_out = down(hidden, mine, both)
+    for group, offsets in enumerate(down_groups):
+        if group:
+            blocks = [b for k in offsets for b in (downs[k], down_twins[k])]
+            first = down(hidden, blocks, len(shifts))
         for index, (dx, dy) in enumerate(shifts):
-            pieces.append(returned(parts_out[index], dx, dy))
-    return finish(stream, pieces, down_groups, length, len(shifts))
+            pieces.append(returned(first[index], dx, dy))
+    earlier = len(shifts) * (len(down_groups) - 1)
+    stream = finish(stream, pieces[:earlier], down_groups[:-1], length, len(shifts))
+    return finish_last(stream, pieces[earlier:], down_groups[-1], length)
 
 
 def groups_of(length):
-    last = length - 1
-    return (
-        (tuple(range(last)), (last,)),
-        (tuple(range(last - 1)), (last - 1, last)),
-    )
+    order = arrivals(length)
+    return (order[:1], order[1:-1], order[-1:])
 
 
 def solution(mesh):

time: 342 us -> 333 us (0.974)
  waiting for transfers between devices: 126 us -> 166 us
  starting transfers between devices: 131 us -> 91.9 us
  Pallas kernels: 75.5 us -> 67.2 us
    ppermute x18 -> x9, starting transfers between devices: 56.9 us -> 14.6 us  [the longest x3 6.22 us: spread(): blocks[length - step] = lax.ppermute(source, 'so', pairs)]
    ppermute x18 -> x9, waiting for transfers between devices: 53.9 us -> 91.3 us  [the longest x3 51.7 us: spread(): blocks[length - step] = lax.ppermute(source, 'so', pairs)]
    ppermute x4 -> x7, starting transfers between devices: 5.84 us -> 41.2 us  [twin(): return lax.ppermute(a, 'ti', [(0, 1), (1, 0)])]
    ppermute x3, starting transfers between devices: 33.9 us -> 8.53 us  [on_device(): state, decay = opened(lax.ppermute(plane, 'so', pairs))]
    ppermute x3, starting transfers between devices: 15.2 us -> 5.27 us  [swapped(): return lax.ppermute(a, ('si', 'ti'), pairs)]
    pallas_call x8 -> x6, Pallas kernels: 53.1 us -> 45.6 us  [the longest x1 21.2 us: make_hidden(): pl.pallas_call(functools.partial(hidden_kernel, length, count), grid=(cou...]
    ppermute x3, waiting for transfers between devices: 0.01 us -> 5.96 us  [dealt(): return lax.ppermute(a, ('to', 'ti'), pairs)]
    ppermute x4, waiting for transfers between devices: 33 us -> 38.8 us  [traded(): return lax.ppermute(a, ('si', 'to', 'ti'), pairs)]
  transfers between devices with their start and end apart: 44 -> 42, of which waited for: 15 -> 19; matrix products, arithmetic and copies ran while one was open for 1% -> 1% of each run, Pallas kernels for 21% -> 18%
where the time goes in v1:
time: 333 us; the launch traced here: 332 us
  waiting for transfers between devices  166 us (50%)
  starting transfers between devices  91.9 us (28%)
  Pallas kernels  67.2 us (20%)
  local copies, waits for them, and re-layouts  3.33 us (1%)
    ppermute x3, waiting for transfers between devices, spread(): blocks[length - step] = lax.ppermute(source, 'so', pairs)  51.7 us
    ppermute x7, starting transfers between devices, twin(): return lax.ppermute(a, 'ti', [(0, 1), (1, 0)])  41.2 us
    ppermute x4, waiting for transfers between devices, traded(): return lax.ppermute(a, ('si', 'to', 'ti'), pairs)  38.8 us
    ppermute x5, waiting for transfers between devices, spread(): blocks[step] = lax.ppermute(blocks[step - 1], 'so', pairs)  28.9 us
    ppermute x12, waiting for transfers between devices, returned(): return lax.ppermute(a, ('si', 'to', 'ti'), pairs)  26 us
    pallas_call x1, Pallas kernels, make_hidden(): pl.pallas_call(functools.partial(hidden_kernel, length, count), grid=(cou...  21.2 us
    ppermute x12, starting transfers between devices, returned(): return lax.ppermute(a, ('si', 'to', 'ti'), pairs)  14.6 us
    pallas_call x2, Pallas kernels, down(): pl.pallas_call(functools.partial(down_kernel, count, len(blocks)), out_sh...  13.5 us
  transfers between devices with their start and end apart: 42, of which 19 were waited for; matrix products, arithmetic and copies ran while one was open for 1% of the time, Pallas kernels for 18%

profile of v1, /device:TPU:0, one launch (start us, length us, event | category | flops | bytes accessed | tf_op | source)
XLA Modules:
  0.0 332.4 jit_solution(15107106928591144668)
XLA Ops:
  12.5 10.7 %collective-permute-done.12.refs_1_.refs_5_ = bf16[256,1408]{1,0:T(8,128)(2,1)S(1)} collective-permute-done((bf16[256,1408]{1,0:T(8,128)(2,1)}, bf16[256,1408]{1,0:T(8,128)(2,1)S(1)}, u32[]{:S(2)}, u32[]{:S(2)}) %collective-permute-start.12) | collective-permute-done | bytes 720928 | tf_op jit(solution)/shard_map/ppermute | solution.py:532
  23.2 19.6 %collective-permute-done.13.refs_2_.refs_6_ = bf16[256,1408]{1,0:T(8,128)(2,1)S(1)} collective-permute-done((bf16[256,1408]{1,0:T(8,128)(2,1)S(1)}, bf16[256,1408]{1,0:T(8,128)(2,1)S(1)}, u32[]{:S(2)}, u32[]{:S(2)}) %collective-permute-start.13) | collective-permute-done | bytes 720928 | tf_op jit(solution)/shard_map/ppermute | solution.py:539
  42.8 11.3 %collective-permute-done.16.refs_4_.refs_9_ = bf16[256,1408]{1,0:T(8,128)(2,1)S(1)} collective-permute-done((bf16[256,1408]{1,0:T(8,128)(2,1)S(1)}, bf16[256,1408]{1,0:T(8,128)(2,1)S(1)}, u32[]{:S(2)}, u32[]{:S(2)}) %collective-permute-start.16) | collective-permute-done | bytes 720928 | tf_op jit(solution)/shard_map/ppermute | solution.py:535
  55.1 16.7 %collective-permute-done.17.refs_5_.refs_10_ = bf16[256,1408]{1,0:T(8,128)(2,1)} collective-permute-done((bf16[256,1408]{1,0:T(8,128)(2,1)S(1)}, bf16[256,1408]{1,0:T(8,128)(2,1)}, u32[]{:S(2)}, u32[]{:S(2)}) %collective-permute-start.17) | collective-permute-done | bytes 720928 | tf_op jit(solution)/shard_map/ppermute | solution.py:539
  71.7 4.3 %pack.1 = bf16[6,256,1408]{2,1,0:T(8,128)(2,1)} custom-call(bf16[256,1408]{1,0:T(8,128)(2,1)} %copy-done, bf16[256,1408]{1,0:T(8,128)(2,1)} %copy-done.2, bf16[256,1408]{1,0:T(8,128)(2,1)} %copy-done.4, bf16[256,1408]{1,0:T(8,128)(2,1)} %copy-done.1, bf16[256,1408]{1,0:T(8,128)(2,1)} %copy-done.5, bf16[256,1408]{1,0:T(8,128)(2,1)} %collective-permute-done.17.refs_5_.refs_10_), custom_call_target="tpu_custom_call" | custom-call | tf_op jit(solution)/shard_map/pack/pallas_call | solution.py:207
  76.3 10.1 %local_scan.1 = (f32[1024,256]{1,0:T(8,128)}, f32[1024,256]{1,0:T(8,128)}, bf16[272,128]{1,0:T(8,128)(2,1)}) custom-call(bf16[1024,256]{1,0:T(8,128)(2,1)} %probe.1, bf16[1024,256]{1,0:T(8,128)(2,1)} %retention.1, bf16[1024,256]{1,0:T(8,128)(2,1)} %content.1, f32[1,256]{1,0:T(1,128)} %bitcast.26, f32[1024,256]{1,0:T(8,128)} %surge.1), custom_call_target="tpu_custom_call" | custom-call | tf_op jit(solution)/shard_map/local_scan/pallas_call | solution.py:102
  94.8 4.6 %collective-permute-start.1 = (bf16[272,128]{1,0:T(8,128)(2,1)S(1)}, bf16[272,128]{1,0:T(8,128)(2,1)S(1)}, u32[]{:S(2)}, u32[]{:S(2)}) collective-permute-start(bf16[272,128]{1,0:T(8,128)(2,1)S(1)} %maximum_maximum_fusion), channel_id=1, source_target_pairs={{0,8},{8,16},{16,24},{1,9},{9,17},{17,25},{2,10},{10,18},{18,26},{... | collective-permute-start | bytes 208904 | tf_op jit(solution)/shard_map/ppermute | solution.py:575
  104.0 6.2 %mix.1 = (bf16[256,256]{1,0:T(8,128)(2,1)}, bf16[256,256]{1,0:T(8,128)(2,1)}, bf16[256,256]{1,0:T(8,128)(2,1)}, bf16[256,256]{1,0:T(8,128)(2,1)}) custom-call(s32[4]{0:T(128)} %add_add_fusion.1.order, f32[1024,256]{1,0:T(8,128)} %get-tuple-element.27.out, f32[1024,256]{1,0:T(8,128)} %get-tuple-element.28.carried, f32[256,128]{1,0:T(8,128)} %fusion.4.state, ...), custom_call_target="tpu_custom_call" | custom-call | tf_op jit(solution)/shard_map/mix/pallas_call | solution.py:136
  112.6 4.2 %collective-permute-done.5.refs_2_ = bf16[256,256]{1,0:T(8,128)(2,1)S(1)} collective-permute-done((bf16[256,256]{1,0:T(8,128)(2,1)}, bf16[256,256]{1,0:T(8,128)(2,1)S(1)}, u32[]{:S(2)}, u32[]{:S(2)}) %collective-permute-start.5) | collective-permute-done | bytes 131104 | tf_op jit(solution)/shard_map/ppermute | solution.py:517
  119.2 5.3 %project.1 = (bf16[256,2048]{1,0:T(8,128)(2,1)}, bf16[256,2048]{1,0:T(8,128)(2,1)}) custom-call(s32[4]{0:T(128)} %add_add_fusion.order, bf16[256,256]{1,0:T(8,128)(2,1)} %get-tuple-element.30.refs_0_, bf16[256,256]{1,0:T(8,128)(2,1)} %copy-done.26, bf16[256,256]{1,0:T(8,128)(2,1)} %copy-done.27, bf16[256,256]{1,0:T(8,128)(2,1)} %copy-done.28, ...), custom_call_target="tpu_custom_call" | custom-call | tf_op jit(solution)/shard_map/project/pallas_call | solution.py:173
  131.0 38.7 %collective-permute-done.8.refs_1_ = bf16[256,2048]{1,0:T(8,128)(2,1)S(1)} collective-permute-done((bf16[256,2048]{1,0:T(8,128)(2,1)}, bf16[256,2048]{1,0:T(8,128)(2,1)S(1)}, u32[]{:S(2)}, u32[]{:S(2)}) %collective-permute-start.8) | collective-permute-done | bytes 1048608 | tf_op jit(solution)/shard_map/ppermute | solution.py:502
  169.7 5.0 %collective-permute-start.23 = (bf16[1408,256]{1,0:T(8,128)(2,1)S(1)}, bf16[1408,256]{1,0:T(8,128)(2,1)S(1)}, u32[]{:S(2)}, u32[]{:S(2)}) collective-permute-start(bf16[1408,256]{1,0:T(8,128)(2,1)S(1)} %collective-permute-done.22.refs_15_), channel_id=1, source_target_pairs={{0,1},{1,0},{2,3},{3,2},{4,5},{5,4},{6,7},{7,6},{8,9},{9,8},{10,11... | collective-permute-start | bytes 2162696 | tf_op jit(solution)/shard_map/ppermute | solution.py:520
  175.2 3.9 %collective-permute-start.18 = (bf16[256,1408]{1,0:T(8,128)(2,1)S(1)}, bf16[256,1408]{1,0:T(8,128)(2,1)S(1)}, u32[]{:S(2)}, u32[]{:S(2)}) collective-permute-start(bf16[256,1408]{1,0:T(8,128)(2,1)S(1)} %copy-done.6), channel_id=1, source_target_pairs={{0,8},{8,16},{16,24},{24,0},{1,9},{9,17},{17,25},{25,1},{2,10},{10... | collective-permute-start | bytes 2162696 | tf_op jit(solution)/shard_map/ppermute | solution.py:535
  179.5 15.6 %collective-permute-start.20 = (bf16[256,1408]{1,0:T(8,128)(2,1)S(1)}, bf16[256,1408]{1,0:T(8,128)(2,1)S(1)}, u32[]{:S(2)}, u32[]{:S(2)}) collective-permute-start(bf16[256,1408]{1,0:T(8,128)(2,1)S(1)} %collective-permute-done.14.refs_7_), channel_id=1, source_target_pairs={{0,1},{1,0},{2,3},{3,2},{4,5},{5,4},{6,7},{7,6},{8,9},{9,8},{10,11... | collective-permute-start | bytes 2162696 | tf_op jit(solution)/shard_map/ppermute | solution.py:520
  195.7 15.3 %collective-permute-done.18.refs_11_ = bf16[256,1408]{1,0:T(8,128)(2,1)S(1)} collective-permute-done((bf16[256,1408]{1,0:T(8,128)(2,1)S(1)}, bf16[256,1408]{1,0:T(8,128)(2,1)S(1)}, u32[]{:S(2)}, u32[]{:S(2)}) %collective-permute-start.18) | collective-permute-done | bytes 720928 | tf_op jit(solution)/shard_map/ppermute | solution.py:535
  211.0 13.3 %collective-permute-start.21 = (bf16[256,1408]{1,0:T(8,128)(2,1)S(1)}, bf16[256,1408]{1,0:T(8,128)(2,1)S(1)}, u32[]{:S(2)}, u32[]{:S(2)}) collective-permute-start(bf16[256,1408]{1,0:T(8,128)(2,1)S(1)} %collective-permute-done.18.refs_11_), channel_id=1, source_target_pairs={{0,1},{1,0},{2,3},{3,2},{4,5},{5,4},{6,7},{7,6},{8,9},{9,8},{10,11... | collective-permute-start | bytes 2162696 | tf_op jit(solution)/shard_map/ppermute | solution.py:520
  224.4 15.4 %collective-permute-done.30.refs_2_ = bf16[1408,256]{1,0:T(8,128)(2,1)} collective-permute-done((bf16[1408,256]{1,0:T(8,128)(2,1)S(1)}, bf16[1408,256]{1,0:T(8,128)(2,1)}, u32[]{:S(2)}, u32[]{:S(2)}) %collective-permute-start.30) | collective-permute-done | bytes 720928 | tf_op jit(solution)/shard_map/ppermute | solution.py:539
  242.0 6.6 %collective-permute-start.37 = (bf16[1408,256]{1,0:T(8,128)(2,1)}, bf16[1408,256]{1,0:T(8,128)(2,1)}, u32[]{:S(2)}, u32[]{:S(2)}) collective-permute-start(bf16[1408,256]{1,0:T(8,128)(2,1)} %collective-permute-done.36.refs_0_), channel_id=1, source_target_pairs={{0,1},{1,0},{2,3},{3,2},{4,5},{5,4},{6,7},{7,6},{8,9},{9,8},{10,11... | collective-permute-start | bytes 2162696 | tf_op jit(solution)/shard_map/ppermute | solution.py:520
  249.4 21.2 %make_hidden.1 = (bf16[1024,1408]{1,0:T(8,128)(2,1)}, bf16[256,512]{1,0:T(8,128)(2,1)}, bf16[256,512]{1,0:T(8,128)(2,1)}, bf16[256,512]{1,0:T(8,128)(2,1)}, bf16[256,512]{1,0:T(8,128)(2,1)}) custom-call(bf16[256,2048]{1,0:T(8,128)(2,1)} %copy-done.7, bf16[256,2048]{1,0:T(8,128)(2,1)} %copy-done.8, bf16[256,2048]{1,0:T(8,128)(2,1)} %copy-done.9, ...), custom_call_target="tpu_custom_call" | custom-call | tf_op jit(solution)/shard_map/make_hidden/pallas_call | solution.py:322
  274.2 7.8 %down.2 = (bf16[256,1024]{1,0:T(8,128)(2,1)}, bf16[256,1024]{1,0:T(8,128)(2,1)}, bf16[256,1024]{1,0:T(8,128)(2,1)}, bf16[256,1024]{1,0:T(8,128)(2,1)}) custom-call(bf16[1024,1408]{1,0:T(8,128)(2,1)} %get-tuple-element.40.hidden, bf16[1408,256]{1,0:T(8,128)(2,1)} %collective-permute-done.28.refs_0_, bf16[1408,256]{1,0:T(8,128)(2,1)} %collective-permute-done.29.refs_1_, ...), custom_call_target="tpu_custom_call" | custom-call | tf_op jit(solution)/shard_map/down/pallas_call | solution.py:367
  288.7 5.7 %down.3 = (bf16[256,512]{1,0:T(8,128)(2,1)}, bf16[256,512]{1,0:T(8,128)(2,1)}, bf16[256,512]{1,0:T(8,128)(2,1)}, bf16[256,512]{1,0:T(8,128)(2,1)}) custom-call(bf16[1024,1408]{1,0:T(8,128)(2,1)} %get-tuple-element.40.hidden, bf16[1408,256]{1,0:T(8,128)(2,1)} %collective-permute-done.36.refs_0_, bf16[1408,256]{1,0:T(8,128)(2,1)} %collective-permute-done.37.refs_1_), custom_call_target="tpu_custom_call" | custom-call | tf_op jit(solution)/shard_map/down/pallas_call | solution.py:367
  294.4 12.3 %collective-permute-done.27.refs_3_ = bf16[256,512]{1,0:T(8,128)(2,1)S(1)} collective-permute-done((bf16[256,512]{1,0:T(8,128)(2,1)S(1)}, bf16[256,512]{1,0:T(8,128)(2,1)S(1)}, u32[]{:S(2)}, u32[]{:S(2)}) %collective-permute-start.27) | collective-permute-done | bytes 262176 | tf_op jit(solution)/shard_map/ppermute | solution.py:511
  311.6 6.4 %collective-permute-done.35.refs_7_ = bf16[256,1024]{1,0:T(8,128)(2,1)S(1)} collective-permute-done((bf16[256,1024]{1,0:T(8,128)(2,1)}, bf16[256,1024]{1,0:T(8,128)(2,1)S(1)}, u32[]{:S(2)}, u32[]{:S(2)}) %collective-permute-start.35) | collective-permute-done | bytes 524320 | tf_op jit(solution)/shard_map/ppermute | solution.py:511
  322.5 6.8 %collective-permute-done.41.refs_3_ = bf16[256,512]{1,0:T(8,128)(2,1)} collective-permute-done((bf16[256,512]{1,0:T(8,128)(2,1)}, bf16[256,512]{1,0:T(8,128)(2,1)}, u32[]{:S(2)}, u32[]{:S(2)}) %collective-permute-start.41) | collective-permute-done | bytes 262176 | tf_op jit(solution)/shard_map/ppermute | solution.py:511
  (142 shorter events, 64.9 us)
Async XLA Ops:
  3.5 19.7 %collective-permute-start.12 = (bf16[256,1408]{1,0:T(8,128)(2,1)}, bf16[256,1408]{1,0:T(8,128)(2,1)S(1)}, u32[]{:S(2)}, u32[]{:S(2)}) collective-permute-start(bf16[256,1408]{1,0:T(8,128)(2,1)} %param.23), channel_id=1, source_target_pairs={{0,8},{1,12},{4,9},{5,13},{8,16},{9,20},{12,17},{13,21},{16,24},{1... | collective-permute-start | bytes 2162696 | tf_op jit(solution)/shard_map/ppermute | solution.py:532
  6.6 36.3 %collective-permute-start.13 = (bf16[256,1408]{1,0:T(8,128)(2,1)S(1)}, bf16[256,1408]{1,0:T(8,128)(2,1)S(1)}, u32[]{:S(2)}, u32[]{:S(2)}) collective-permute-start(bf16[256,1408]{1,0:T(8,128)(2,1)S(1)} %collective-permute-done.11.refs_0_.refs_4_), channel_id=1, source_target_pairs={{8,0},{16,8},{24,16},{0,24},{9,1},{17,9},{25,17},{1,25},{10,2},{18... | collective-permute-start | bytes 2162696 | tf_op jit(solution)/shard_map/ppermute | solution.py:539
  8.7 45.5 %collective-permute-start.16 = (bf16[256,1408]{1,0:T(8,128)(2,1)S(1)}, bf16[256,1408]{1,0:T(8,128)(2,1)S(1)}, u32[]{:S(2)}, u32[]{:S(2)}) collective-permute-start(bf16[256,1408]{1,0:T(8,128)(2,1)S(1)} %collective-permute-done.15.refs_3_.refs_8_), channel_id=1, source_target_pairs={{0,8},{8,16},{16,24},{24,0},{1,9},{9,17},{17,25},{25,1},{2,10},{10... | collective-permute-start | bytes 2162696 | tf_op jit(solution)/shard_map/ppermute | solution.py:535
  8.7 63.1 %collective-permute-start.17 = (bf16[256,1408]{1,0:T(8,128)(2,1)S(1)}, bf16[256,1408]{1,0:T(8,128)(2,1)}, u32[]{:S(2)}, u32[]{:S(2)}) collective-permute-start(bf16[256,1408]{1,0:T(8,128)(2,1)S(1)} %collective-permute-done.15.refs_3_.refs_8_), channel_id=1, source_target_pairs={{8,0},{16,8},{24,16},{0,24},{9,1},{17,9},{25,17},{1,25},{10,2},{18... | collective-permute-start | bytes 2162696 | tf_op jit(solution)/shard_map/ppermute | solution.py:539
  76.1 173.3 %collective-permute-start.19 = (bf16[6,256,1408]{2,1,0:T(8,128)(2,1)}, bf16[6,256,1408]{2,1,0:T(8,128)(2,1)}, u32[]{:S(2)}, u32[]{:S(2)}) collective-permute-start(bf16[6,256,1408]{2,1,0:T(8,128)(2,1)} %pack.1), channel_id=1, source_target_pairs={{0,1},{1,0},{2,3},{3,2},{4,5},{5,4},{6,7},{7,6},{8,9},{9,8},{10,11... | collective-permute-start | bytes 12976136 | tf_op jit(solution)/shard_map/ppermute | solution.py:520
  86.7 43.2 %collective-permute-start.22 = (bf16[1408,256]{1,0:T(8,128)(2,1)}, bf16[1408,256]{1,0:T(8,128)(2,1)S(1)}, u32[]{:S(2)}, u32[]{:S(2)}) collective-permute-start(bf16[1408,256]{1,0:T(8,128)(2,1)} %param.25), channel_id=1, source_target_pairs={{0,0},{1,4},{4,1},{5,5},{2,2},{3,6},{6,3},{7,7},{8,8},{9,12},{12,9... | collective-permute-start | bytes 2162696 | tf_op jit(solution)/shard_map/ppermute | solution.py:493
  126.4 43.3 %collective-permute-start.8 = (bf16[256,2048]{1,0:T(8,128)(2,1)}, bf16[256,2048]{1,0:T(8,128)(2,1)S(1)}, u32[]{:S(2)}, u32[]{:S(2)}) collective-permute-start(bf16[256,2048]{1,0:T(8,128)(2,1)} %get-tuple-element.35), channel_id=1, source_target_pairs={{0,4},{1,0},{2,6},{3,2},{4,5},{5,1},{6,7},{7,3},{8,12},{9,8},{10,1... | collective-permute-start | bytes 3145736 | tf_op jit(solution)/shard_map/ppermute | solution.py:502
  128.4 46.3 %collective-permute-start.9 = (bf16[256,2048]{1,0:T(8,128)(2,1)}, bf16[256,2048]{1,0:T(8,128)(2,1)S(1)}, u32[]{:S(2)}, u32[]{:S(2)}) collective-permute-start(bf16[256,2048]{1,0:T(8,128)(2,1)} %get-tuple-element.35), channel_id=1, source_target_pairs={{0,2},{1,6},{2,0},{3,4},{4,3},{5,7},{6,1},{7,5},{8,10},{9,14},{10,... | collective-permute-start | bytes 3145736 | tf_op jit(solution)/shard_map/ppermute | solution.py:502
  129.9 45.3 %collective-permute-start.10 = (bf16[256,2048]{1,0:T(8,128)(2,1)}, bf16[256,2048]{1,0:T(8,128)(2,1)S(1)}, u32[]{:S(2)}, u32[]{:S(2)}) collective-permute-start(bf16[256,2048]{1,0:T(8,128)(2,1)} %get-tuple-element.35), channel_id=1, source_target_pairs={{0,6},{1,2},{2,4},{3,0},{4,7},{5,3},{6,5},{7,1},{8,14},{9,10},{10,... | collective-permute-start | bytes 3145736 | tf_op jit(solution)/shard_map/ppermute | solution.py:502
  130.0 49.1 %collective-permute-start.14 = (bf16[256,1408]{1,0:T(8,128)(2,1)S(1)}, bf16[256,1408]{1,0:T(8,128)(2,1)S(1)}, u32[]{:S(2)}, u32[]{:S(2)}) collective-permute-start(bf16[256,1408]{1,0:T(8,128)(2,1)S(1)} %copy-done.3), channel_id=1, source_target_pairs={{0,8},{8,16},{16,24},{24,0},{1,9},{9,17},{17,25},{25,1},{2,10},{10... | collective-permute-start | bytes 2162696 | tf_op jit(solution)/shard_map/ppermute | solution.py:535
  174.7 21.0 %collective-permute-start.28 = (bf16[1408,256]{1,0:T(8,128)(2,1)S(1)}, bf16[1408,256]{1,0:T(8,128)(2,1)}, u32[]{:S(2)}, u32[]{:S(2)}) collective-permute-start(bf16[1408,256]{1,0:T(8,128)(2,1)S(1)} %collective-permute-done.22.refs_15_), channel_id=1, source_target_pairs={{0,8},{8,16},{16,24},{24,0},{1,9},{9,17},{17,25},{25,1},{2,10},{10... | collective-permute-start | bytes 2162696 | tf_op jit(solution)/shard_map/ppermute | solution.py:535
  175.2 35.8 %collective-permute-start.18 = (bf16[256,1408]{1,0:T(8,128)(2,1)S(1)}, bf16[256,1408]{1,0:T(8,128)(2,1)S(1)}, u32[]{:S(2)}, u32[]{:S(2)}) collective-permute-start(bf16[256,1408]{1,0:T(8,128)(2,1)S(1)} %copy-done.6), channel_id=1, source_target_pairs={{0,8},{8,16},{16,24},{24,0},{1,9},{9,17},{17,25},{25,1},{2,10},{10... | collective-permute-start | bytes 2162696 | tf_op jit(solution)/shard_map/ppermute | solution.py:535
  179.2 60.6 %collective-permute-start.30 = (bf16[1408,256]{1,0:T(8,128)(2,1)S(1)}, bf16[1408,256]{1,0:T(8,128)(2,1)}, u32[]{:S(2)}, u32[]{:S(2)}) collective-permute-start(bf16[1408,256]{1,0:T(8,128)(2,1)S(1)} %collective-permute-done.22.refs_15_), channel_id=1, source_target_pairs={{8,0},{16,8},{24,16},{0,24},{9,1},{17,9},{25,17},{1,25},{10,2},{18... | collective-permute-start | bytes 2162696 | tf_op jit(solution)/shard_map/ppermute | solution.py:539
  179.5 60.7 %collective-permute-start.20 = (bf16[256,1408]{1,0:T(8,128)(2,1)S(1)}, bf16[256,1408]{1,0:T(8,128)(2,1)S(1)}, u32[]{:S(2)}, u32[]{:S(2)}) collective-permute-start(bf16[256,1408]{1,0:T(8,128)(2,1)S(1)} %collective-permute-done.14.refs_7_), channel_id=1, source_target_pairs={{0,1},{1,0},{2,3},{3,2},{4,5},{5,4},{6,7},{7,6},{8,9},{9,8},{10,11... | collective-permute-start | bytes 2162696 | tf_op jit(solution)/shard_map/ppermute | solution.py:520
  195.7 46.3 %collective-permute-start.36 = (bf16[1408,256]{1,0:T(8,128)(2,1)}, bf16[1408,256]{1,0:T(8,128)(2,1)}, u32[]{:S(2)}, u32[]{:S(2)}) collective-permute-start(bf16[1408,256]{1,0:T(8,128)(2,1)} %collective-permute-done.28.refs_0_), channel_id=1, source_target_pairs={{0,8},{8,16},{16,24},{24,0},{1,9},{9,17},{17,25},{25,1},{2,10},{10... | collective-permute-start | bytes 2162696 | tf_op jit(solution)/shard_map/ppermute | solution.py:535
  211.0 37.5 %collective-permute-start.21 = (bf16[256,1408]{1,0:T(8,128)(2,1)S(1)}, bf16[256,1408]{1,0:T(8,128)(2,1)S(1)}, u32[]{:S(2)}, u32[]{:S(2)}) collective-permute-start(bf16[256,1408]{1,0:T(8,128)(2,1)S(1)} %collective-permute-done.18.refs_11_), channel_id=1, source_target_pairs={{0,1},{1,0},{2,3},{3,2},{4,5},{5,4},{6,7},{7,6},{8,9},{9,8},{10,11... | collective-permute-start | bytes 2162696 | tf_op jit(solution)/shard_map/ppermute | solution.py:520
  239.8 32.9 %collective-permute-start.29 = (bf16[1408,256]{1,0:T(8,128)(2,1)}, bf16[1408,256]{1,0:T(8,128)(2,1)}, u32[]{:S(2)}, u32[]{:S(2)}) collective-permute-start(bf16[1408,256]{1,0:T(8,128)(2,1)} %collective-permute-done.28.refs_0_), channel_id=1, source_target_pairs={{0,1},{1,0},{2,3},{3,2},{4,5},{5,4},{6,7},{7,6},{8,9},{9,8},{10,11... | collective-permute-start | bytes 2162696 | tf_op jit(solution)/shard_map/ppermute | solution.py:520
  240.1 34.1 %collective-permute-start.31 = (bf16[1408,256]{1,0:T(8,128)(2,1)}, bf16[1408,256]{1,0:T(8,128)(2,1)}, u32[]{:S(2)}, u32[]{:S(2)}) collective-permute-start(bf16[1408,256]{1,0:T(8,128)(2,1)} %collective-permute-done.30.refs_2_), channel_id=1, source_target_pairs={{0,1},{1,0},{2,3},{3,2},{4,5},{5,4},{6,7},{7,6},{8,9},{9,8},{10,11... | collective-permute-start | bytes 2162696 | tf_op jit(solution)/shard_map/ppermute | solution.py:520
  242.0 41.8 %collective-permute-start.37 = (bf16[1408,256]{1,0:T(8,128)(2,1)}, bf16[1408,256]{1,0:T(8,128)(2,1)}, u32[]{:S(2)}, u32[]{:S(2)}) collective-permute-start(bf16[1408,256]{1,0:T(8,128)(2,1)} %collective-permute-done.36.refs_0_), channel_id=1, source_target_pairs={{0,1},{1,0},{2,3},{3,2},{4,5},{5,4},{6,7},{7,6},{8,9},{9,8},{10,11... | collective-permute-start | bytes 2162696 | tf_op jit(solution)/shard_map/ppermute | solution.py:520
  282.1 26.3 %collective-permute-start.32 = (bf16[256,1024]{1,0:T(8,128)(2,1)}, bf16[256,1024]{1,0:T(8,128)(2,1)S(1)}, u32[]{:S(2)}, u32[]{:S(2)}) collective-permute-start(bf16[256,1024]{1,0:T(8,128)(2,1)} %get-tuple-element.41), channel_id=1, source_target_pairs={{0,0},{4,1},{2,2},{6,3},{1,4},{5,5},{3,6},{7,7},{8,8},{12,9},{10,1... | collective-permute-start | bytes 1572872 | tf_op jit(solution)/shard_map/ppermute | solution.py:511
  283.8 26.0 %collective-permute-start.33 = (bf16[256,1024]{1,0:T(8,128)(2,1)}, bf16[256,1024]{1,0:T(8,128)(2,1)S(1)}, u32[]{:S(2)}, u32[]{:S(2)}) collective-permute-start(bf16[256,1024]{1,0:T(8,128)(2,1)} %get-tuple-element.42), channel_id=1, source_target_pairs={{4,0},{0,1},{6,2},{2,3},{5,4},{1,5},{7,6},{3,7},{12,8},{8,9},{14,1... | collective-permute-start | bytes 1572872 | tf_op jit(solution)/shard_map/ppermute | solution.py:511
  285.5 24.8 %collective-permute-start.34 = (bf16[256,1024]{1,0:T(8,128)(2,1)}, bf16[256,1024]{1,0:T(8,128)(2,1)S(1)}, u32[]{:S(2)}, u32[]{:S(2)}) collective-permute-start(bf16[256,1024]{1,0:T(8,128)(2,1)} %get-tuple-element.43), channel_id=1, source_target_pairs={{2,0},{6,1},{0,2},{4,3},{3,4},{7,5},{1,6},{5,7},{10,8},{14,9},{8,1... | collective-permute-start | bytes 1572872 | tf_op jit(solution)/shard_map/ppermute | solution.py:511
  286.1 20.7 %collective-permute-start.27 = (bf16[256,512]{1,0:T(8,128)(2,1)S(1)}, bf16[256,512]{1,0:T(8,128)(2,1)S(1)}, u32[]{:S(2)}, u32[]{:S(2)}) collective-permute-start(bf16[256,512]{1,0:T(8,128)(2,1)S(1)} %copy-done.29), channel_id=1, source_target_pairs={{6,0},{2,1},{4,2},{0,3},{7,4},{3,5},{5,6},{1,7},{14,8},{10,9},{12,... | collective-permute-start | bytes 786440 | tf_op jit(solution)/shard_map/ppermute | solution.py:511
  288.5 29.5 %collective-permute-start.35 = (bf16[256,1024]{1,0:T(8,128)(2,1)}, bf16[256,1024]{1,0:T(8,128)(2,1)S(1)}, u32[]{:S(2)}, u32[]{:S(2)}) collective-permute-start(bf16[256,1024]{1,0:T(8,128)(2,1)} %get-tuple-element.44), channel_id=1, source_target_pairs={{6,0},{2,1},{4,2},{0,3},{7,4},{3,5},{5,6},{1,7},{14,8},{10,9},{12,... | collective-permute-start | bytes 1572872 | tf_op jit(solution)/shard_map/ppermute | solution.py:511
  (48 other events, 1188.2 us)

commit v2 on v1

--- a/solution.py
+++ b/solution.py
@@ -12,7 +12,8 @@
 HEAD_DIM = 128
 BLOCK = 64
 CHUNK = 512
-ROOM = 66_000_000
+SPAN = 256
+ROOM = 67_000_000
 EPSILON = 1e-06
 F32 = jnp.float32
 BF16 = jnp.bfloat16
@@ -40,7 +41,61 @@
     return dot(a_high, b_high, dims) + (dot(a_high, b_low, dims) + dot(a_low, b_high, dims))
 
 
-def scan_kernel(probe, retention, content, slack, surge, out, carried, message, state, offset):
+def exact_sums(ones, rate):
+    high = rate.astype(BF16)
+    rest = rate - high.astype(F32)
+    middle = rest.astype(BF16)
+    low = (rest - middle.astype(F32)).astype(BF16)
+    return dot(ones, high) + (dot(ones, middle) + dot(ones, low))
+
+
+def state_kernel(retention, content, slack, surge, message, state, offset):
+    rows, width = retention.shape
+    heads = width // HEAD_DIM
+    span = min(SPAN, rows)
+    first = lax.broadcasted_iota(jnp.int32, (span, span), 0)
+    second = lax.broadcasted_iota(jnp.int32, (span, span), 1)
+    later = jnp.where(second > first, 1.0, 0.0).astype(BF16)
+    state[...] = jnp.zeros_like(state)
+    offset[...] = jnp.zeros_like(offset)
+    for turn in range(rows // span):
+        here = slice(turn * span, (turn + 1) * span)
+        gate = slack[...] * jax.nn.sigmoid(-retention[here, :].astype(F32))
+        rate = jnp.log1p(-gate) + surge[here, :]
+        following = exact_sums(later, rate)
+        leave_high, leave_low = parts(gate * jnp.exp(following))
+        total = following[0:1, :] + rate[0:1, :]
+        decay = jnp.exp(total)
+        for head in range(heads):
+            lanes = slice(head * HEAD_DIM, (head + 1) * HEAD_DIM)
+            values = content[here, lanes]
+            state[lanes, :] = decay[:, lanes] * state[lanes, :] + (
+                dot(values, leave_high[:, lanes], TN) + dot(values, leave_low[:, lanes], TN)
+            )
+        offset[...] += total
+    message[0:width, :] = state[...].astype(BF16)
+    final = jnp.exp(offset[...])
+    tail = jnp.concatenate(
+        [final[:, h * HEAD_DIM : (h + 1) * HEAD_DIM] for h in range(heads)]
+        + [jnp.zeros((16 - heads, HEAD_DIM), F32)],
+        axis=0,
+    )
+    message[width : width + 16, :] = tail.astype(BF16)
+
+
+def passed_on(retention, content, slack, surge):
+    width = retention.shape[1]
+    return pl.pallas_call(
+        state_kernel,
+        out_shape=jax.ShapeDtypeStruct((width + 16, HEAD_DIM), BF16),
+        in_specs=[VMEM] * 4,
+        out_specs=VMEM,
+        scratch_shapes=[pltpu.VMEM((width, HEAD_DIM), F32), pltpu.VMEM((1, width), F32)],
+        name="passed_on",
+    )(retention, content, slack.reshape(1, width), surge)
+
+
+def scan_kernel(probe, retention, content, slack, surge, out, carried, state, offset):
     rows, width = probe.shape
     heads = width // HEAD_DIM
     state[...] = jnp.zeros_like(state)
@@ -57,11 +112,7 @@
         gate = slack[...] * jax.nn.sigmoid(-retention[here, :].astype(F32))
         rate = jnp.log1p(-gate) + surge[here, :]
         value = content[here, :]
-        high = rate.astype(BF16)
-        rest = rate - high.astype(F32)
-        middle_part = rest.astype(BF16)
-        low = (rest - middle_part.astype(F32)).astype(BF16)
-        cumulative = dot(ones, high) + (dot(ones, middle_part) + dot(ones, low))
+        cumulative = exact_sums(ones, rate)
         middle = cumulative[BLOCK // 2 : BLOCK // 2 + 1, :]
         total = cumulative[BLOCK - 1 : BLOCK, :]
         left = query * jnp.exp(cumulative - middle)
@@ -87,14 +138,6 @@
         return 0
 
     lax.fori_loop(0, rows // BLOCK, step, 0, unroll=4)
-    message[0:width, :] = state[...].astype(BF16)
-    final = jnp.exp(offset[...])
-    tail = jnp.concatenate(
-        [final[:, h * HEAD_DIM : (h + 1) * HEAD_DIM] for h in range(heads)]
-        + [jnp.zeros((16 - heads, HEAD_DIM), F32)],
-        axis=0,
-    )
-    message[width : width + 16, :] = tail.astype(BF16)
 
 
 def local_scan(probe, retention, content, slack, surge):
@@ -104,10 +147,9 @@
         out_shape=(
             jax.ShapeDtypeStruct((rows, width), F32),
             jax.ShapeDtypeStruct((rows, width), F32),
-            jax.ShapeDtypeStruct((width + 16, HEAD_DIM), BF16),
         ),
         in_specs=[VMEM] * 5,
-        out_specs=(VMEM, VMEM, VMEM),
+        out_specs=(VMEM, VMEM),
         scratch_shapes=[pltpu.VMEM((width, HEAD_DIM), F32), pltpu.VMEM((1, width), F32)],
         name="local_scan",
     )(probe, retention, content, slack.reshape(1, width), surge)
@@ -190,34 +232,10 @@
     return lax.rem(line - offset + length, length)
 
 
-def pack_kernel(*refs):
-    blocks, (packed, sems) = refs[:-2], refs[-2:]
-    copies = [
-        pltpu.make_async_copy(block, packed.at[index], sems.at[index])
-        for index, block in enumerate(blocks)
-    ]
-    for copy in copies:
-        copy.start()
-    for copy in copies:
-        copy.wait()
-
-
-def pack(blocks):
-    count = len(blocks)
-    return pl.pallas_call(
-        pack_kernel,
-        out_shape=jax.ShapeDtypeStruct((count,) + blocks[0].shape, BF16),
-        in_specs=[ANY] * count,
-        out_specs=VMEM,
-        scratch_shapes=[pltpu.SemaphoreType.DMA((count,))],
-        name="pack",
-    )(*blocks)
-
-
-def hidden_kernel(length, count, *refs):
+def hidden_kernel(length, count, own_normed, *refs):
     normed, refs = refs[:count], refs[count:]
-    gates, ups, refs = refs[:length], refs[length : 2 * length], refs[2 * length :]
-    (packed, last_gate, last_up, down_own, down_twin), refs = refs[:5], refs[5:]
+    gates, ups, refs = refs[: 2 * length], refs[2 * length : 4 * length], refs[4 * length :]
+    (down_own, down_twin), refs = refs[:2], refs[2:]
     hidden, outs, refs = refs[0], refs[1 : 1 + count], refs[1 + count :]
     rows_now, gate_all, up_all, down_all, gate_sum, up_sum, sems, piece_sem = refs
     depth, units = gates[0].shape
@@ -225,7 +243,6 @@
     line = lax.axis_index("so")
     core = lax.axis_index("ti")
     turn = pl.program_id(0)
-    early = length - 1
 
     height = normed[0].shape[0]
     group = hidden.shape[0] // height
@@ -236,13 +253,11 @@
     for twin in range(2):
         side = 1 - core if twin else core
         for index, offset in enumerate(arrivals(length)):
-            if not twin:
-                gate_block, up_block = gates[index], ups[index]
-            elif index < early:
-                gate_block, up_block = packed.at[index], packed.at[early + index]
-            else:
-                gate_block, up_block = last_gate, last_up
             slot = twin * length + index
+            gate_block, up_block = gates[slot], ups[slot]
+            if gate_block.shape[0] > depth:
+                gate_block = gate_block.at[pl.ds(0, depth), :]
+                up_block = up_block.at[pl.ds(depth, depth), :]
             rows = pl.ds(slot * depth, depth)
             weight_copies += [
                 pltpu.make_async_copy(gate_block, gate_all.at[rows, :], sems.at[2 * slot]),
@@ -256,10 +271,11 @@
         for index, block in enumerate((down_own, down_twin))
     ]
 
-    def piece_copies(piece):
+    def piece_copies(piece, source=None):
+        source = normed[piece] if source is None else source
         return [
             pltpu.make_async_copy(
-                normed[piece].at[:, pl.ds(pl.multiple_of(place * depth, depth), depth)],
+                source.at[:, pl.ds(pl.multiple_of(place * depth, depth), depth)],
                 rows_now.at[pl.ds(piece * height, height), pl.ds(slot * depth, depth)],
                 piece_sem.at[piece * 2 * length + slot],
             )
@@ -270,9 +286,21 @@
 
     @pl.when(turn == 0)
     def _():
+        stays = lax.axis_index("si") == core
+
+        @pl.when(stays)
+        def _():
+            for copy in piece_copies(0, own_normed):
+                copy.start()
+
+        @pl.when(jnp.logical_not(stays))
+        def _():
+            for copy in piece_copies(0):
+                copy.start()
+
         first = [copy for piece in range(group) for copy in piece_copies(piece)]
         others = [copy for piece in range(group, count) for copy in piece_copies(piece)]
-        for copy in first + weight_copies + down_copies + others:
+        for copy in first[2 * length :] + weight_copies + down_copies + others:
             copy.start()
         for copy in first + weight_copies[: 2 * length]:
             copy.wait()
@@ -313,9 +341,9 @@
             outs[index][...] = share[start : start + height, :]
 
 
-def make_hidden(normed, gates, ups, packed, last_gate, last_up, down_own, down_twin):
+def make_hidden(own_normed, normed, gates, ups, down_own, down_twin):
     rows, features = normed[0].shape
-    length = len(gates)
+    length = len(gates) // 2
     units = gates[0].shape[1]
     columns = 2 * down_own.shape[1]
     count = len(normed)
@@ -324,7 +352,7 @@
         grid=(count // 2,),
         out_shape=[jax.ShapeDtypeStruct((count * rows, units), BF16)]
         + [jax.ShapeDtypeStruct((rows, columns), BF16)] * count,
-        in_specs=[ANY] * (count + 2 * length + 5),
+        in_specs=[ANY] * (1 + count + 4 * length + 2),
         out_specs=[pl.BlockSpec((2 * rows, units), lambda i: (i, 0))]
         + [pl.BlockSpec((rows, columns), lambda i: (0, 0))] * count,
         scratch_shapes=[
@@ -339,7 +367,7 @@
         ],
         compiler_params=pltpu.CompilerParams(vmem_limit_bytes=ROOM),
         name="make_hidden",
-    )(*normed, *gates, *ups, packed, last_gate, last_up, down_own, down_twin)
+    )(own_normed, *normed, *gates, *ups, down_own, down_twin)
 
 
 def down_kernel(count, blocks, hidden, *refs):
@@ -377,13 +405,21 @@
     )(hidden, *blocks)
 
 
+def summed(pieces, lanes):
+    stays = lax.axis_index("si") == lax.axis_index("ti")
+    total = jnp.where(stays, pieces[0][:, lanes].astype(F32), pieces[1][:, lanes].astype(F32))
+    for piece in pieces[2:]:
+        total = total + piece[:, lanes].astype(F32)
+    return total
+
+
 def finish_kernel(length, groups, count, stream, *refs):
     pieces, out = refs[:-1], refs[-1]
     columns = stream.shape[1] // (2 * length)
     line = lax.axis_index("so")
     side = lax.axis_index("si")
     for group, offsets in enumerate(groups):
-        mine = pieces[group * count : (group + 1) * count]
+        mine = pieces[group * (count + 1) : (group + 1) * (count + 1)]
         for index, offset in enumerate(offsets):
             for twin in range(2):
                 place = column_place(line, offset, length)
@@ -391,9 +427,7 @@
                 lanes = pl.ds(pl.multiple_of(block * columns, columns), columns)
                 start = (2 * index + twin) * columns
                 local = slice(start, start + columns)
-                total = mine[0][:, local].astype(F32)
-                for piece in mine[1:]:
-                    total = total + piece[:, local].astype(F32)
+                total = summed(mine, local)
                 out[:, lanes] = (stream[:, lanes].astype(F32) + total).astype(BF16)
 
 
@@ -432,9 +466,7 @@
         read.start()
     for slot, (read, write) in enumerate(moves):
         local = slice(slot * columns, (slot + 1) * columns)
-        total = pieces[0][:, local].astype(F32)
-        for piece in pieces[1:]:
-            total = total + piece[:, local].astype(F32)
+        total = summed(pieces, local)
         read.wait()
         done[slot] = (held[slot].astype(F32) + total).astype(BF16)
         write.start()
@@ -499,6 +531,7 @@
             for x in range(ring)
             for c in range(2)
         ]
+        pairs = [(source, target) for source, target in pairs if source != target]
         return lax.ppermute(a, ("si", "to", "ti"), pairs)
 
     def returned(a, dx, dy):
@@ -508,6 +541,7 @@
             for x in range(ring)
             for c in range(2)
         ]
+        pairs = [(source, target) for source, target in pairs if source != target]
         return lax.ppermute(a, ("si", "to", "ti"), pairs)
 
     def dealt(a, dx, dc):
@@ -541,9 +575,11 @@
 
     gates = spread(swapped(switch_matrix), switch_matrix)
     ups = spread(swapped(expansion_matrix))
-    downs = spread(swapped(contraction_matrix))
-
-    out, carried, message = local_scan(
+    moved = lax.ppermute(contraction_matrix, ("si", "ti"), [(1, 2), (2, 1)])
+    downs = spread(jnp.where(side == core, contraction_matrix, moved))
+
+    message = passed_on(retention_preactivation, content_vector, retention_slack, surge_rate)
+    out, carried = local_scan(
         probe_preactivation,
         retention_preactivation,
         content_vector,
@@ -594,24 +630,25 @@
         skip_stream_vector,
         mlp_scaling_factor,
     )
+    own_normed = normed
     normed = [traded(normed, dx, dy) for dx, dy in shifts]
 
-    gates = [gates[offset] for offset in order]
-    ups = [ups[offset] for offset in order]
-    packed = pack(gates[:-1] + ups[:-1])
-    packed = twin(packed)
+    both = twin(jnp.concatenate([gates[0], ups[0]]))
+    later = order[1:]
+    gates = [gates[k] for k in order] + [both] + [twin(gates[k]) for k in later]
+    ups = [ups[k] for k in order] + [both] + [twin(ups[k]) for k in later]
     down_twins = [twin(block) for block in downs]
-    last_twins = twin(gates[-1]), twin(ups[-1])
-    hidden, *first = make_hidden(normed, gates, ups, packed, *last_twins, downs[0], down_twins[0])
+    hidden, *first = make_hidden(own_normed, normed, gates, ups, downs[0], down_twins[0])
 
     pieces = []
     for group, offsets in enumerate(down_groups):
         if group:
             blocks = [b for k in offsets for b in (downs[k], down_twins[k])]
             first = down(hidden, blocks, len(shifts))
+        pieces.append(first[0])
         for index, (dx, dy) in enumerate(shifts):
             pieces.append(returned(first[index], dx, dy))
-    earlier = len(shifts) * (len(down_groups) - 1)
+    earlier = (len(shifts) + 1) * (len(down_groups) - 1)
     stream = finish(stream, pieces[:earlier], down_groups[:-1], length, len(shifts))
     return finish_last(stream, pieces[earlier:], down_groups[-1], length)
 

time: 333 us -> 316 us (0.949)
  waiting for transfers between devices: 166 us -> 87.4 us
  starting transfers between devices: 91.9 us -> 154 us
    ppermute x7 -> x11, starting transfers between devices: 41.2 us -> 93.7 us  [twin(): return lax.ppermute(a, 'ti', [(0, 1), (1, 0)])]
    ppermute x3, waiting for transfers between devices: 51.7 us -> 11.6 us  [spread(): blocks[length - step] = lax.ppermute(source, 'so', pairs)]
    ppermute x5, waiting for transfers between devices: 28.9 us -> 7.26 us  [spread(): blocks[step] = lax.ppermute(blocks[step - 1], 'so', pairs)]
    ppermute x1, waiting for transfers between devices: 10.7 us -> 0.01 us  [spread(): blocks[step] = lax.ppermute(held, ('so', 'si', 'ti'), pairs)]
    ppermute x3, starting transfers between devices: 6.22 us -> 11.4 us  [spread(): blocks[length - step] = lax.ppermute(source, 'so', pairs)]
  transfers between devices with their start and end apart: 42 -> 46, of which waited for: 19 -> 11; matrix products, arithmetic and copies ran while one was open for 1% -> 1% of each run, Pallas kernels for 18% -> 19%
where the time goes in v2:
time: 316 us; the launch traced here: 315 us
  starting transfers between devices  154 us (49%)
  waiting for transfers between devices  87.4 us (28%)
  Pallas kernels  67.5 us (21%)
  other arithmetic  3.28 us (1%)
    ppermute x11, starting transfers between devices, twin(): return lax.ppermute(a, 'ti', [(0, 1), (1, 0)])  93.7 us
    ppermute x4, waiting for transfers between devices, traded(): return lax.ppermute(a, ('si', 'to', 'ti'), pairs)  36.5 us
    ppermute x12, waiting for transfers between devices, returned(): return lax.ppermute(a, ('si', 'to', 'ti'), pairs)  25.6 us
    pallas_call x1, Pallas kernels, make_hidden(): pl.pallas_call(functools.partial(hidden_kernel, length, count), grid=(cou...  21.1 us
    ppermute x12, starting transfers between devices, returned(): return lax.ppermute(a, ('si', 'to', 'ti'), pairs)  14.9 us
    pallas_call x2, Pallas kernels, down(): pl.pallas_call(functools.partial(down_kernel, count, len(blocks)), out_sh...  13.5 us
    ppermute x3, waiting for transfers between devices, spread(): blocks[length - step] = lax.ppermute(source, 'so', pairs)  11.6 us
    ppermute x3, starting transfers between devices, spread(): blocks[length - step] = lax.ppermute(source, 'so', pairs)  11.4 us
  transfers between devices with their start and end apart: 46, of which 11 were waited for; matrix products, arithmetic and copies ran while one was open for 1% of the time, Pallas kernels for 19%

profile of v2, /device:TPU:0, one launch (start us, length us, event | category | flops | bytes accessed | tf_op | source)
XLA Modules:
  0.0 314.8 jit_solution(11102363681246697760)
XLA Ops:
  0.0 4.3 %passed_on.1 = bf16[272,128]{1,0:T(8,128)(2,1)} custom-call(bf16[1024,256]{1,0:T(8,128)(2,1)} %retention.3, bf16[1024,256]{1,0:T(8,128)(2,1)} %content.3, f32[1,256]{1,0:T(1,128)} %bitcast.26, f32[1024,256]{1,0:T(8,128)} %surge.3), custom_call_target="tpu_custom_call" | custom-call | tf_op jit(solution)/shard_map/passed_on/pallas_call | solution.py:88
  12.4 10.1 %local_scan.1 = (f32[1024,256]{1,0:T(8,128)}, f32[1024,256]{1,0:T(8,128)}) custom-call(bf16[1024,256]{1,0:T(8,128)(2,1)} %probe.1, bf16[1024,256]{1,0:T(8,128)(2,1)} %retention.3, bf16[1024,256]{1,0:T(8,128)(2,1)} %content.3, f32[1,256]{1,0:T(1,128)} %bitcast.27, f32[1024,256]{1,0:T(8,128)} %surge.3), custom_call_target="tpu_custom_call" | custom-call | tf_op jit(solution)/shard_map/local_scan/pallas_call | solution.py:145
  23.7 4.5 %collective-permute-start.2 = (bf16[272,128]{1,0:T(8,128)(2,1)S(1)}, bf16[272,128]{1,0:T(8,128)(2,1)S(1)}, u32[]{:S(2)}, u32[]{:S(2)}) collective-permute-start(bf16[272,128]{1,0:T(8,128)(2,1)S(1)} %maximum_maximum_fusion), channel_id=1, source_target_pairs={{0,16},{8,24},{1,17},{9,25},{2,18},{10,26},{3,19},{11,27},{4,20},{... | collective-permute-start | bytes 208904 | tf_op jit(solution)/shard_map/ppermute | solution.py:611
  31.0 4.0 %collective-permute-start.3 = (bf16[272,128]{1,0:T(8,128)(2,1)S(1)}, bf16[272,128]{1,0:T(8,128)(2,1)S(1)}, u32[]{:S(2)}, u32[]{:S(2)}) collective-permute-start(bf16[272,128]{1,0:T(8,128)(2,1)S(1)} %maximum_maximum_fusion), channel_id=1, source_target_pairs={{0,24},{1,25},{2,26},{3,27},{4,28},{5,29},{6,30},{7,31}} | collective-permute-start | bytes 208904 | tf_op jit(solution)/shard_map/ppermute | solution.py:611
  37.9 6.0 %mix.1 = (bf16[256,256]{1,0:T(8,128)(2,1)}, bf16[256,256]{1,0:T(8,128)(2,1)}, bf16[256,256]{1,0:T(8,128)(2,1)}, bf16[256,256]{1,0:T(8,128)(2,1)}) custom-call(s32[4]{0:T(128)} %add_add_fusion.1.order, f32[1024,256]{1,0:T(8,128)} %get-tuple-element.26.out, f32[1024,256]{1,0:T(8,128)} %get-tuple-element.27.carried, f32[256,128]{1,0:T(8,128)} %fusion.4.state, ...), custom_call_target="tpu_custom_call" | custom-call | tf_op jit(solution)/shard_map/mix/pallas_call | solution.py:178
  54.1 5.3 %project.1 = (bf16[256,2048]{1,0:T(8,128)(2,1)}, bf16[256,2048]{1,0:T(8,128)(2,1)}) custom-call(s32[4]{0:T(128)} %add_add_fusion.order, bf16[256,256]{1,0:T(8,128)(2,1)} %get-tuple-element.28.refs_0_, bf16[256,256]{1,0:T(8,128)(2,1)} %copy-done.26, bf16[256,256]{1,0:T(8,128)(2,1)} %copy-done.27, bf16[256,256]{1,0:T(8,128)(2,1)} %copy-done.28, ...), custom_call_target="tpu_custom_call" | custom-call | tf_op jit(solution)/shard_map/project/pallas_call | solution.py:215
  67.0 4.2 %collective-permute-start.13 = (bf16[256,1408]{1,0:T(8,128)(2,1)S(1)}, bf16[256,1408]{1,0:T(8,128)(2,1)S(1)}, u32[]{:S(2)}, u32[]{:S(2)}) collective-permute-start(bf16[256,1408]{1,0:T(8,128)(2,1)S(1)} %collective-permute-done.11.refs_4_), channel_id=1, source_target_pairs={{8,0},{16,8},{24,16},{0,24},{9,1},{17,9},{25,17},{1,25},{10,2},{18... | collective-permute-start | bytes 2162696 | tf_op jit(solution)/shard_map/ppermute | solution.py:573
  71.3 36.5 %collective-permute-done.8.refs_1_ = bf16[256,2048]{1,0:T(8,128)(2,1)S(1)} collective-permute-done((bf16[256,2048]{1,0:T(8,128)(2,1)}, bf16[256,2048]{1,0:T(8,128)(2,1)S(1)}, u32[]{:S(2)}, u32[]{:S(2)}) %collective-permute-start.8) | collective-permute-done | bytes 1048608 | tf_op jit(solution)/shard_map/ppermute | solution.py:535
  107.8 13.7 %collective-permute-start.16 = (bf16[512,1408]{1,0:T(8,128)(2,1)S(1)}, bf16[512,1408]{1,0:T(8,128)(2,1)}, u32[]{:S(2)}, u32[]{:S(2)}) collective-permute-start(bf16[512,1408]{1,0:T(8,128)(2,1)S(1)} %pad_maximum_fusion), channel_id=1, source_target_pairs={{0,1},{1,0},{2,3},{3,2},{4,5},{5,4},{6,7},{7,6},{8,9},{9,8},{10,11... | collective-permute-start | bytes 4325384 | tf_op jit(solution)/shard_map/ppermute | solution.py:554
  121.8 3.9 %collective-permute-start.21 = (bf16[256,1408]{1,0:T(8,128)(2,1)S(1)}, bf16[256,1408]{1,0:T(8,128)(2,1)S(1)}, u32[]{:S(2)}, u32[]{:S(2)}) collective-permute-start(bf16[256,1408]{1,0:T(8,128)(2,1)S(1)} %collective-permute-done.15.refs_12_), channel_id=1, source_target_pairs={{8,0},{16,8},{24,16},{0,24},{9,1},{17,9},{25,17},{1,25},{10,2},{18... | collective-permute-start | bytes 2162696 | tf_op jit(solution)/shard_map/ppermute | solution.py:573
  125.6 26.3 %collective-permute-start.27 = (bf16[1408,256]{1,0:T(8,128)(2,1)S(1)}, bf16[1408,256]{1,0:T(8,128)(2,1)S(1)}, u32[]{:S(2)}, u32[]{:S(2)}) collective-permute-start(bf16[1408,256]{1,0:T(8,128)(2,1)S(1)} %broadcast_select_fusion.refs_20_), channel_id=1, source_target_pairs={{0,1},{1,0},{2,3},{3,2},{4,5},{5,4},{6,7},{7,6},{8,9},{9,8},{10,11... | collective-permute-start | bytes 2162696 | tf_op jit(solution)/shard_map/ppermute | solution.py:554
  157.7 9.7 %collective-permute-done.21.refs_14_ = bf16[256,1408]{1,0:T(8,128)(2,1)S(1)} collective-permute-done((bf16[256,1408]{1,0:T(8,128)(2,1)S(1)}, bf16[256,1408]{1,0:T(8,128)(2,1)S(1)}, u32[]{:S(2)}, u32[]{:S(2)}) %collective-permute-start.21) | collective-permute-done | bytes 720928 | tf_op jit(solution)/shard_map/ppermute | solution.py:573
  167.4 13.6 %collective-permute-start.18 = (bf16[256,1408]{1,0:T(8,128)(2,1)S(1)}, bf16[256,1408]{1,0:T(8,128)(2,1)S(1)}, u32[]{:S(2)}, u32[]{:S(2)}) collective-permute-start(bf16[256,1408]{1,0:T(8,128)(2,1)S(1)} %collective-permute-done.13.refs_6_), channel_id=1, source_target_pairs={{0,1},{1,0},{2,3},{3,2},{4,5},{5,4},{6,7},{7,6},{8,9},{9,8},{10,11... | collective-permute-start | bytes 2162696 | tf_op jit(solution)/shard_map/ppermute | solution.py:554
  181.0 15.4 %collective-permute-start.19 = (bf16[256,1408]{1,0:T(8,128)(2,1)S(1)}, bf16[256,1408]{1,0:T(8,128)(2,1)S(1)}, u32[]{:S(2)}, u32[]{:S(2)}) collective-permute-start(bf16[256,1408]{1,0:T(8,128)(2,1)S(1)} %collective-permute-done.14.refs_7_), channel_id=1, source_target_pairs={{0,1},{1,0},{2,3},{3,2},{4,5},{5,4},{6,7},{7,6},{8,9},{9,8},{10,11... | collective-permute-start | bytes 2162696 | tf_op jit(solution)/shard_map/ppermute | solution.py:554
  198.3 8.6 %collective-permute-start.23 = (bf16[256,1408]{1,0:T(8,128)(2,1)S(1)}, bf16[256,1408]{1,0:T(8,128)(2,1)S(1)}, u32[]{:S(2)}, u32[]{:S(2)}) collective-permute-start(bf16[256,1408]{1,0:T(8,128)(2,1)S(1)} %collective-permute-done.20.refs_13_), channel_id=1, source_target_pairs={{0,1},{1,0},{2,3},{3,2},{4,5},{5,4},{6,7},{7,6},{8,9},{9,8},{10,11... | collective-permute-start | bytes 2162696 | tf_op jit(solution)/shard_map/ppermute | solution.py:554
  207.3 13.4 %collective-permute-start.25 = (bf16[256,1408]{1,0:T(8,128)(2,1)S(1)}, bf16[256,1408]{1,0:T(8,128)(2,1)}, u32[]{:S(2)}, u32[]{:S(2)}) collective-permute-start(bf16[256,1408]{1,0:T(8,128)(2,1)S(1)} %collective-permute-done.22.refs_15_), channel_id=1, source_target_pairs={{0,1},{1,0},{2,3},{3,2},{4,5},{5,4},{6,7},{7,6},{8,9},{9,8},{10,11... | collective-permute-start | bytes 2162696 | tf_op jit(solution)/shard_map/ppermute | solution.py:554
  221.4 7.3 %collective-permute-done.40.refs_0_ = bf16[1408,256]{1,0:T(8,128)(2,1)} collective-permute-done((bf16[1408,256]{1,0:T(8,128)(2,1)}, bf16[1408,256]{1,0:T(8,128)(2,1)}, u32[]{:S(2)}, u32[]{:S(2)}) %collective-permute-start.40) | collective-permute-done | bytes 720928 | tf_op jit(solution)/shard_map/ppermute | solution.py:569
  231.5 21.1 %make_hidden.1 = (bf16[1024,1408]{1,0:T(8,128)(2,1)}, bf16[256,512]{1,0:T(8,128)(2,1)}, bf16[256,512]{1,0:T(8,128)(2,1)}, bf16[256,512]{1,0:T(8,128)(2,1)}, bf16[256,512]{1,0:T(8,128)(2,1)}) custom-call(bf16[256,2048]{1,0:T(8,128)(2,1)} %get-tuple-element.33.own_normed, bf16[256,2048]{1,0:T(8,128)(2,1)} %copy-done.3, bf16[256,2048]{1,0:T(8,128)(2,1)} %copy-done.4, ...), custom_call_target="tpu_custom_call" | custom-call | tf_op jit(solution)/shard_map/make_hidden/pallas_call | solution.py:350
  258.4 7.9 %down.2 = (bf16[256,1024]{1,0:T(8,128)(2,1)}, bf16[256,1024]{1,0:T(8,128)(2,1)}, bf16[256,1024]{1,0:T(8,128)(2,1)}, bf16[256,1024]{1,0:T(8,128)(2,1)}) custom-call(bf16[1024,1408]{1,0:T(8,128)(2,1)} %get-tuple-element.38.hidden, bf16[1408,256]{1,0:T(8,128)(2,1)} %collective-permute-done.32.refs_0_, bf16[1408,256]{1,0:T(8,128)(2,1)} %collective-permute-done.33.refs_1_, ...), custom_call_target="tpu_custom_call" | custom-call | tf_op jit(solution)/shard_map/down/pallas_call | solution.py:395
  271.1 5.7 %down.3 = (bf16[256,512]{1,0:T(8,128)(2,1)}, bf16[256,512]{1,0:T(8,128)(2,1)}, bf16[256,512]{1,0:T(8,128)(2,1)}, bf16[256,512]{1,0:T(8,128)(2,1)}) custom-call(bf16[1024,1408]{1,0:T(8,128)(2,1)} %get-tuple-element.38.hidden, bf16[1408,256]{1,0:T(8,128)(2,1)} %collective-permute-done.40.refs_0_, bf16[1408,256]{1,0:T(8,128)(2,1)} %collective-permute-done.41.refs_1_), custom_call_target="tpu_custom_call" | custom-call | tf_op jit(solution)/shard_map/down/pallas_call | solution.py:395
  276.8 14.0 %collective-permute-done.31.refs_4_ = bf16[256,512]{1,0:T(8,128)(2,1)S(1)} collective-permute-done((bf16[256,512]{1,0:T(8,128)(2,1)S(1)}, bf16[256,512]{1,0:T(8,128)(2,1)S(1)}, u32[]{:S(2)}, u32[]{:S(2)}) %collective-permute-start.31) | collective-permute-done | bytes 262176 | tf_op jit(solution)/shard_map/ppermute | solution.py:545
  295.1 6.9 %collective-permute-done.39.refs_9_ = bf16[256,1024]{1,0:T(8,128)(2,1)S(1)} collective-permute-done((bf16[256,1024]{1,0:T(8,128)(2,1)}, bf16[256,1024]{1,0:T(8,128)(2,1)S(1)}, u32[]{:S(2)}, u32[]{:S(2)}) %collective-permute-start.39) | collective-permute-done | bytes 524320 | tf_op jit(solution)/shard_map/ppermute | solution.py:545
  302.8 4.0 %finish.1.stream = bf16[256,2048]{1,0:T(8,128)(2,1)} custom-call(bf16[256,2048]{1,0:T(8,128)(2,1)} %get-tuple-element.32.stream_ref, bf16[256,512]{1,0:T(8,128)(2,1)} %get-tuple-element.34.refs_0_, bf16[256,512]{1,0:T(8,128)(2,1)} %copy-done.21, bf16[256,512]{1,0:T(8,128)(2,1)} %copy-done.22, bf16[256,512]{1,0:T(8,128)(2,1)} %copy-done.23, ...), custom_call_target="tpu_custom_call" | custom-call | tf_op jit(solution)/shard_map/finish/pallas_call | solution.py:439
  307.1 4.5 %collective-permute-done.45.refs_4_ = bf16[256,512]{1,0:T(8,128)(2,1)} collective-permute-done((bf16[256,512]{1,0:T(8,128)(2,1)}, bf16[256,512]{1,0:T(8,128)(2,1)}, u32[]{:S(2)}, u32[]{:S(2)}) %collective-permute-start.45) | collective-permute-done | bytes 262176 | tf_op jit(solution)/shard_map/ppermute | solution.py:545
  (152 shorter events, 63.4 us)
Async XLA Ops:
  7.3 56.1 %collective-permute-start.11 = (bf16[256,1408]{1,0:T(8,128)(2,1)}, bf16[256,1408]{1,0:T(8,128)(2,1)S(1)}, u32[]{:S(2)}, u32[]{:S(2)}) collective-permute-start(bf16[256,1408]{1,0:T(8,128)(2,1)} %param.23), channel_id=1, source_target_pairs={{0,0},{1,4},{4,1},{5,5},{2,2},{3,6},{6,3},{7,7},{8,8},{9,12},{12,9... | collective-permute-start | bytes 2162696 | tf_op jit(solution)/shard_map/ppermute | solution.py:525
  9.1 56.1 %collective-permute-start.12 = (bf16[256,1408]{1,0:T(8,128)(2,1)}, bf16[256,1408]{1,0:T(8,128)(2,1)}, u32[]{:S(2)}, u32[]{:S(2)}) collective-permute-start(bf16[256,1408]{1,0:T(8,128)(2,1)} %param.23), channel_id=1, source_target_pairs={{0,8},{1,12},{4,9},{5,13},{8,16},{9,20},{12,17},{13,21},{16,24},{1... | collective-permute-start | bytes 2162696 | tf_op jit(solution)/shard_map/ppermute | solution.py:566
  10.7 54.7 %collective-permute-start.15 = (bf16[256,1408]{1,0:T(8,128)(2,1)}, bf16[256,1408]{1,0:T(8,128)(2,1)S(1)}, u32[]{:S(2)}, u32[]{:S(2)}) collective-permute-start(bf16[256,1408]{1,0:T(8,128)(2,1)} %param.24), channel_id=1, source_target_pairs={{0,0},{1,4},{4,1},{5,5},{2,2},{3,6},{6,3},{7,7},{8,8},{9,12},{12,9... | collective-permute-start | bytes 2162696 | tf_op jit(solution)/shard_map/ppermute | solution.py:525
  60.1 47.6 %collective-permute-start.8 = (bf16[256,2048]{1,0:T(8,128)(2,1)}, bf16[256,2048]{1,0:T(8,128)(2,1)S(1)}, u32[]{:S(2)}, u32[]{:S(2)}) collective-permute-start(bf16[256,2048]{1,0:T(8,128)(2,1)} %get-tuple-element.33.own_normed), channel_id=1, source_target_pairs={{0,4},{1,0},{2,6},{3,2},{4,5},{5,1},{6,7},{7,3},{8,12},{9,8},{10,1... | collective-permute-start | bytes 3145736 | tf_op jit(solution)/shard_map/ppermute | solution.py:535
  63.4 58.1 %collective-permute-start.9 = (bf16[256,2048]{1,0:T(8,128)(2,1)}, bf16[256,2048]{1,0:T(8,128)(2,1)}, u32[]{:S(2)}, u32[]{:S(2)}) collective-permute-start(bf16[256,2048]{1,0:T(8,128)(2,1)} %get-tuple-element.33.own_normed), channel_id=1, source_target_pairs={{0,2},{1,6},{2,0},{3,4},{4,3},{5,7},{6,1},{7,5},{8,10},{9,14},{10,... | collective-permute-start | bytes 3145736 | tf_op jit(solution)/shard_map/ppermute | solution.py:535
  65.2 56.4 %collective-permute-start.10 = (bf16[256,2048]{1,0:T(8,128)(2,1)}, bf16[256,2048]{1,0:T(8,128)(2,1)}, u32[]{:S(2)}, u32[]{:S(2)}) collective-permute-start(bf16[256,2048]{1,0:T(8,128)(2,1)} %get-tuple-element.33.own_normed), channel_id=1, source_target_pairs={{0,6},{1,2},{2,4},{3,0},{4,7},{5,3},{6,5},{7,1},{8,14},{9,10},{10,... | collective-permute-start | bytes 3145736 | tf_op jit(solution)/shard_map/ppermute | solution.py:535
  67.0 54.8 %collective-permute-start.13 = (bf16[256,1408]{1,0:T(8,128)(2,1)S(1)}, bf16[256,1408]{1,0:T(8,128)(2,1)S(1)}, u32[]{:S(2)}, u32[]{:S(2)}) collective-permute-start(bf16[256,1408]{1,0:T(8,128)(2,1)S(1)} %collective-permute-done.11.refs_4_), channel_id=1, source_target_pairs={{8,0},{16,8},{24,16},{0,24},{9,1},{17,9},{25,17},{1,25},{10,2},{18... | collective-permute-start | bytes 2162696 | tf_op jit(solution)/shard_map/ppermute | solution.py:573
  71.2 54.5 %collective-permute-start.14 = (bf16[256,1408]{1,0:T(8,128)(2,1)}, bf16[256,1408]{1,0:T(8,128)(2,1)S(1)}, u32[]{:S(2)}, u32[]{:S(2)}) collective-permute-start(bf16[256,1408]{1,0:T(8,128)(2,1)} %collective-permute-done.12.refs_5_), channel_id=1, source_target_pairs={{0,8},{8,16},{16,24},{24,0},{1,9},{9,17},{17,25},{25,1},{2,10},{10... | collective-permute-start | bytes 2162696 | tf_op jit(solution)/shard_map/ppermute | solution.py:569
  107.8 99.1 %collective-permute-start.16 = (bf16[512,1408]{1,0:T(8,128)(2,1)S(1)}, bf16[512,1408]{1,0:T(8,128)(2,1)}, u32[]{:S(2)}, u32[]{:S(2)}) collective-permute-start(bf16[512,1408]{1,0:T(8,128)(2,1)S(1)} %pad_maximum_fusion), channel_id=1, source_target_pairs={{0,1},{1,0},{2,3},{3,2},{4,5},{5,4},{6,7},{7,6},{8,9},{9,8},{10,11... | collective-permute-start | bytes 4325384 | tf_op jit(solution)/shard_map/ppermute | solution.py:554
  121.5 30.4 %collective-permute-start.17 = (bf16[256,1408]{1,0:T(8,128)(2,1)}, bf16[256,1408]{1,0:T(8,128)(2,1)S(1)}, u32[]{:S(2)}, u32[]{:S(2)}) collective-permute-start(bf16[256,1408]{1,0:T(8,128)(2,1)} %collective-permute-done.12.refs_5_), channel_id=1, source_target_pairs={{0,1},{1,0},{2,3},{3,2},{4,5},{5,4},{6,7},{7,6},{8,9},{9,8},{10,11... | collective-permute-start | bytes 2162696 | tf_op jit(solution)/shard_map/ppermute | solution.py:554
  121.6 32.7 %collective-permute-start.20 = (bf16[256,1408]{1,0:T(8,128)(2,1)S(1)}, bf16[256,1408]{1,0:T(8,128)(2,1)S(1)}, u32[]{:S(2)}, u32[]{:S(2)}) collective-permute-start(bf16[256,1408]{1,0:T(8,128)(2,1)S(1)} %collective-permute-done.15.refs_12_), channel_id=1, source_target_pairs={{0,8},{8,16},{16,24},{24,0},{1,9},{9,17},{17,25},{25,1},{2,10},{10... | collective-permute-start | bytes 2162696 | tf_op jit(solution)/shard_map/ppermute | solution.py:569
  121.8 45.6 %collective-permute-start.21 = (bf16[256,1408]{1,0:T(8,128)(2,1)S(1)}, bf16[256,1408]{1,0:T(8,128)(2,1)S(1)}, u32[]{:S(2)}, u32[]{:S(2)}) collective-permute-start(bf16[256,1408]{1,0:T(8,128)(2,1)S(1)} %collective-permute-done.15.refs_12_), channel_id=1, source_target_pairs={{8,0},{16,8},{24,16},{0,24},{9,1},{17,9},{25,17},{1,25},{10,2},{18... | collective-permute-start | bytes 2162696 | tf_op jit(solution)/shard_map/ppermute | solution.py:573
  125.6 55.3 %collective-permute-start.27 = (bf16[1408,256]{1,0:T(8,128)(2,1)S(1)}, bf16[1408,256]{1,0:T(8,128)(2,1)S(1)}, u32[]{:S(2)}, u32[]{:S(2)}) collective-permute-start(bf16[1408,256]{1,0:T(8,128)(2,1)S(1)} %broadcast_select_fusion.refs_20_), channel_id=1, source_target_pairs={{0,1},{1,0},{2,3},{3,2},{4,5},{5,4},{6,7},{7,6},{8,9},{9,8},{10,11... | collective-permute-start | bytes 2162696 | tf_op jit(solution)/shard_map/ppermute | solution.py:554
  151.9 29.1 %collective-permute-start.32 = (bf16[1408,256]{1,0:T(8,128)(2,1)S(1)}, bf16[1408,256]{1,0:T(8,128)(2,1)}, u32[]{:S(2)}, u32[]{:S(2)}) collective-permute-start(bf16[1408,256]{1,0:T(8,128)(2,1)S(1)} %broadcast_select_fusion.refs_20_), channel_id=1, source_target_pairs={{0,8},{8,16},{16,24},{24,0},{1,9},{9,17},{17,25},{25,1},{2,10},{10... | collective-permute-start | bytes 2162696 | tf_op jit(solution)/shard_map/ppermute | solution.py:569
  154.3 44.0 %collective-permute-start.34 = (bf16[1408,256]{1,0:T(8,128)(2,1)S(1)}, bf16[1408,256]{1,0:T(8,128)(2,1)}, u32[]{:S(2)}, u32[]{:S(2)}) collective-permute-start(bf16[1408,256]{1,0:T(8,128)(2,1)S(1)} %broadcast_select_fusion.refs_20_), channel_id=1, source_target_pairs={{8,0},{16,8},{24,16},{0,24},{9,1},{17,9},{25,17},{1,25},{10,2},{18... | collective-permute-start | bytes 2162696 | tf_op jit(solution)/shard_map/ppermute | solution.py:573
  167.4 39.8 %collective-permute-start.18 = (bf16[256,1408]{1,0:T(8,128)(2,1)S(1)}, bf16[256,1408]{1,0:T(8,128)(2,1)S(1)}, u32[]{:S(2)}, u32[]{:S(2)}) collective-permute-start(bf16[256,1408]{1,0:T(8,128)(2,1)S(1)} %collective-permute-done.13.refs_6_), channel_id=1, source_target_pairs={{0,1},{1,0},{2,3},{3,2},{4,5},{5,4},{6,7},{7,6},{8,9},{9,8},{10,11... | collective-permute-start | bytes 2162696 | tf_op jit(solution)/shard_map/ppermute | solution.py:554
  181.0 26.3 %collective-permute-start.22 = (bf16[256,1408]{1,0:T(8,128)(2,1)S(1)}, bf16[256,1408]{1,0:T(8,128)(2,1)S(1)}, u32[]{:S(2)}, u32[]{:S(2)}) collective-permute-start(bf16[256,1408]{1,0:T(8,128)(2,1)S(1)} %collective-permute-done.20.refs_13_), channel_id=1, source_target_pairs={{0,8},{8,16},{16,24},{24,0},{1,9},{9,17},{17,25},{25,1},{2,10},{10... | collective-permute-start | bytes 2162696 | tf_op jit(solution)/shard_map/ppermute | solution.py:569
  181.0 39.7 %collective-permute-start.19 = (bf16[256,1408]{1,0:T(8,128)(2,1)S(1)}, bf16[256,1408]{1,0:T(8,128)(2,1)S(1)}, u32[]{:S(2)}, u32[]{:S(2)}) collective-permute-start(bf16[256,1408]{1,0:T(8,128)(2,1)S(1)} %collective-permute-done.14.refs_7_), channel_id=1, source_target_pairs={{0,1},{1,0},{2,3},{3,2},{4,5},{5,4},{6,7},{7,6},{8,9},{9,8},{10,11... | collective-permute-start | bytes 2162696 | tf_op jit(solution)/shard_map/ppermute | solution.py:554
  220.7 36.2 %collective-permute-start.33 = (bf16[1408,256]{1,0:T(8,128)(2,1)}, bf16[1408,256]{1,0:T(8,128)(2,1)}, u32[]{:S(2)}, u32[]{:S(2)}) collective-permute-start(bf16[1408,256]{1,0:T(8,128)(2,1)} %collective-permute-done.32.refs_0_), channel_id=1, source_target_pairs={{0,1},{1,0},{2,3},{3,2},{4,5},{5,4},{6,7},{7,6},{8,9},{9,8},{10,11... | collective-permute-start | bytes 2162696 | tf_op jit(solution)/shard_map/ppermute | solution.py:554
  220.8 37.6 %collective-permute-start.35 = (bf16[1408,256]{1,0:T(8,128)(2,1)}, bf16[1408,256]{1,0:T(8,128)(2,1)}, u32[]{:S(2)}, u32[]{:S(2)}) collective-permute-start(bf16[1408,256]{1,0:T(8,128)(2,1)} %collective-permute-done.34.refs_2_), channel_id=1, source_target_pairs={{0,1},{1,0},{2,3},{3,2},{4,5},{5,4},{6,7},{7,6},{8,9},{9,8},{10,11... | collective-permute-start | bytes 2162696 | tf_op jit(solution)/shard_map/ppermute | solution.py:554
  228.6 38.4 %collective-permute-start.41 = (bf16[1408,256]{1,0:T(8,128)(2,1)}, bf16[1408,256]{1,0:T(8,128)(2,1)}, u32[]{:S(2)}, u32[]{:S(2)}) collective-permute-start(bf16[1408,256]{1,0:T(8,128)(2,1)} %collective-permute-done.40.refs_0_), channel_id=1, source_target_pairs={{0,1},{1,0},{2,3},{3,2},{4,5},{5,4},{6,7},{7,6},{8,9},{9,8},{10,11... | collective-permute-start | bytes 2162696 | tf_op jit(solution)/shard_map/ppermute | solution.py:554
  266.3 25.1 %collective-permute-start.36 = (bf16[256,1024]{1,0:T(8,128)(2,1)}, bf16[256,1024]{1,0:T(8,128)(2,1)S(1)}, u32[]{:S(2)}, u32[]{:S(2)}) collective-permute-start(bf16[256,1024]{1,0:T(8,128)(2,1)} %get-tuple-element.39.refs_5_), channel_id=1, source_target_pairs={{4,1},{6,3},{1,4},{3,6},{12,9},{14,11},{9,12},{11,14},{20,17},{22,... | collective-permute-start | bytes 1572872 | tf_op jit(solution)/shard_map/ppermute | solution.py:545
  267.0 25.2 %collective-permute-start.37 = (bf16[256,1024]{1,0:T(8,128)(2,1)}, bf16[256,1024]{1,0:T(8,128)(2,1)S(1)}, u32[]{:S(2)}, u32[]{:S(2)}) collective-permute-start(bf16[256,1024]{1,0:T(8,128)(2,1)} %get-tuple-element.40), channel_id=1, source_target_pairs={{4,0},{0,1},{6,2},{2,3},{5,4},{1,5},{7,6},{3,7},{12,8},{8,9},{14,1... | collective-permute-start | bytes 1572872 | tf_op jit(solution)/shard_map/ppermute | solution.py:545
  270.8 31.2 %collective-permute-start.39 = (bf16[256,1024]{1,0:T(8,128)(2,1)}, bf16[256,1024]{1,0:T(8,128)(2,1)S(1)}, u32[]{:S(2)}, u32[]{:S(2)}) collective-permute-start(bf16[256,1024]{1,0:T(8,128)(2,1)} %get-tuple-element.42), channel_id=1, source_target_pairs={{6,0},{2,1},{4,2},{0,3},{7,4},{3,5},{5,6},{1,7},{14,8},{10,9},{12,... | collective-permute-start | bytes 1572872 | tf_op jit(solution)/shard_map/ppermute | solution.py:545
  (52 other events, 1550.5 us)
